TPU v7x, 256 devices: a whole 4x4x8 slice. The times are simulated.
256 devices in a mesh: sp: 32 (over z, x), tp: 8 (over y, core).
Axes of the slice: x: 4, y: 4, z: 8, core: 2. Of those that a mesh axis runs over, the one named last changes fastest.
Arguments:
- latent: bfloat16 [73728, 2048], P(('sp', 'tp')), may hold values from -0.6 to 0.6
- context: bfloat16 [256, 2048], P(('sp', 'tp')), may hold values from -6 to 6
- condition: float32 [2048], P('sp'), may hold values from -6 to 6
- context_condition: float32 [2048], P('sp'), may hold values from -6 to 6
- modulation_weight: bfloat16 [2048, 6144], P('sp', 'tp'), may hold values from -0.1875 to 0.1875
- norm_gain: float32 [2048], replicated, may hold values from 0.1 to 1.9
- query_weight: bfloat16 [2048, 1024], replicated
- key_weight: bfloat16 [2048, 256], replicated
- value_weight: bfloat16 [2048, 256], replicated, may hold values from -0.125 to 0.125
- output_weight: bfloat16 [1024, 2048], replicated, may hold values from -0.1875 to 0.1875
- query_gain: float32 [128], replicated, may hold values from 0.5 to 6
- key_gain: float32 [128], replicated, may hold values from 0.5 to 6
- sink_logit: float32 [8], replicated, may hold values from 1 to 5
Outputs:
- updated: bfloat16 [73728, 2048], P(('sp', 'tp'))
All inputs are finite; a program needn't handle non-finite values.
Results may differ from a plain program's by a relative error of at most 0.006.
The roundings to bfloat16 on the way count: a program that leaves them out, or rounds other values in their place, can miss the bound.
Values may be sent and summed in bfloat16 or wider, within the bound.
No kernel may reach another device: no remote copies, remote signals or barrier semaphores. Data moves between devices by JAX's collectives and lax.ppermute only.
A program may use at most 64 MiB of HBM per device.

v0:
```python
import jax
import jax.numpy as jnp
from jax import lax
from jax.sharding import Mesh
from jax.sharding import PartitionSpec as P

WINDOW = 128
GRID_W = 64
SP = ("sp_0", "sp_1")
TP = ("tp_0", "tp_1")
SP_TP = ("sp_0", "sp_1", "tp_0", "tp_1")


EPS = 1e-06
ROPE_BASE = 10000.0
FAR_LOGIT = -1e30


def copy_for_each(array, axis):
    copies = jnp.broadcast_to(array, (lax.axis_size(axis), *array.shape))
    return lax.all_to_all(copies, axis, split_axis=0, concat_axis=0, tiled=True)


def of_everyone(array, axis):
    return copy_for_each(array, axis).sum(axis=0)


def in_order(pieces, dim):
    shape = list(pieces.shape[1:])
    shape[dim] *= pieces.shape[0]
    return jnp.moveaxis(pieces, 0, dim).reshape(shape)


def gather_directly(array, axis, dim):
    pieces = copy_for_each(array, axis)
    return in_order(pieces, dim)


def padded(array, sides, width):
    edges = {}
    for axis, dim in sides:
        size, length = (lax.axis_size(axis), array.shape[dim])
        up = [(i, (i + 1) % size) for i in range(size - 1)]
        last = lax.slice_in_dim(array, length - width, length, axis=dim)
        first = lax.slice_in_dim(array, 0, width, axis=dim)
        edges[dim] = (
            lax.ppermute(last, axis, up),
            lax.ppermute(first, axis, [(b, a) for a, b in up]),
        )
    done = []
    for _, dim in sides:
        low, high = edges[dim]
        around = [(width, width) if d in done else (0, 0) for d in range(array.ndim)]
        array = jnp.concatenate([jnp.pad(low, around), array, jnp.pad(high, around)], axis=dim)
        done.append(dim)
    return array


def whole_of(array, axes, dim):
    far, near = axes
    first = copy_for_each(array, far)
    pieces = jnp.swapaxes(copy_for_each(first, near), 0, 1)
    return in_order(pieces.reshape(-1, *array.shape), dim)


def rms_rows(values_in):
    return values_in * lax.rsqrt(jnp.mean(values_in * values_in, axis=-1, keepdims=True) + EPS)


def turn_halves(halves_in):
    former, latter = jnp.split(halves_in, 2, axis=-1)
    return jnp.concatenate([-latter, former], axis=-1)


def rotary(values_in, positions):
    quarter = values_in.shape[-1] // 4
    inverse = jnp.power(ROPE_BASE, -jnp.arange(quarter, dtype=jnp.float32) / quarter)
    by_rows = (positions // GRID_W).astype(jnp.float32)[:, None] * inverse
    by_cols = (positions % GRID_W).astype(jnp.float32)[:, None] * inverse
    angles = jnp.concatenate([by_rows, by_rows, by_cols, by_cols], axis=-1)[:, None, :]
    row_half, col_half = jnp.split(values_in, 2, axis=-1)
    turned = jnp.concatenate([turn_halves(row_half), turn_halves(col_half)], axis=-1)
    return values_in * jnp.cos(angles) + turned * jnp.sin(angles)


def head_norm(flat, gain):
    per_head = flat.reshape(flat.shape[0], flat.shape[1] // gain.shape[0], gain.shape[0])
    return rms_rows(per_head) * gain


def modulated(tokens_in, norm_gain, shift, scale):
    values_in = tokens_in.astype(jnp.float32)
    return (rms_rows(values_in) * norm_gain * (1.0 + scale) + shift).astype(jnp.bfloat16)


def key_value_rows(hidden_rows, positions, key_weight, value_weight, key_gain):
    row_count = hidden_rows.shape[0]
    kv_width = key_weight.shape[1]
    keys = (
        rotary(
            head_norm(
                jnp.dot(hidden_rows, key_weight, preferred_element_type=jnp.float32), key_gain
            ),
            positions,
        )
        .astype(jnp.bfloat16)
        .reshape(row_count, kv_width)
    )
    values = jnp.dot(hidden_rows, value_weight, preferred_element_type=jnp.float32).astype(
        jnp.bfloat16
    )
    return jnp.stack([keys, values])


def attend(queries, keys, values, ctx_keys, ctx_values, sink_logit, allowed, head_size):
    row_count = queries.shape[0]
    kv_count = keys.shape[1] // head_size
    group = queries.shape[1] // keys.shape[1]
    score_scale = head_size ** (-0.5)
    grouped = queries.reshape(row_count, kv_count, group, head_size)
    near_keys = keys.reshape(keys.shape[0], kv_count, head_size)
    near_values = values.reshape(values.shape[0], kv_count, head_size)
    far_keys = ctx_keys.reshape(ctx_keys.shape[0], kv_count, head_size)
    far_values = ctx_values.reshape(ctx_values.shape[0], kv_count, head_size)
    near_scores = (
        jnp.einsum("rhgd,khd->hgrk", grouped, near_keys, preferred_element_type=jnp.float32)
        * score_scale
    )
    near_scores = jnp.where(allowed, near_scores, FAR_LOGIT)
    ctx_scores = (
        jnp.einsum("rhgd,khd->hgrk", grouped, far_keys, preferred_element_type=jnp.float32)
        * score_scale
    )
    sink_part = sink_logit.reshape(kv_count, group)[:, :, None, None]
    row_max = jnp.maximum(
        jnp.maximum(
            jnp.max(near_scores, axis=-1, keepdims=True),
            jnp.max(ctx_scores, axis=-1, keepdims=True),
        ),
        sink_part,
    )
    near_exp = jnp.exp(near_scores - row_max)
    ctx_exp = jnp.exp(ctx_scores - row_max)
    denominator = (
        jnp.sum(near_exp, axis=-1, keepdims=True)
        + jnp.sum(ctx_exp, axis=-1, keepdims=True)
        + jnp.exp(sink_part - row_max)
    )
    near_probs = (near_exp / denominator).astype(jnp.bfloat16)
    ctx_probs = (ctx_exp / denominator).astype(jnp.bfloat16)
    mixed = jnp.einsum(
        "hgrk,khd->rhgd", near_probs, near_values, preferred_element_type=jnp.float32
    ) + jnp.einsum("hgrk,khd->rhgd", ctx_probs, far_values, preferred_element_type=jnp.float32)
    return mixed.astype(jnp.bfloat16).reshape(row_count, queries.shape[1])


def local(
    latent,
    context,
    condition,
    context_condition,
    modulation_weight,
    norm_gain,
    query_weight,
    key_weight,
    value_weight,
    output_weight,
    query_gain,
    key_gain,
    sink_logit,
):
    model_width = latent.shape[1]
    head_size = query_gain.shape[0]
    kv_width = key_weight.shape[1]
    query_width = query_weight.shape[1]
    activations = jax.nn.silu(jnp.stack([condition, context_condition])).astype(jnp.bfloat16)
    partial_value = jnp.dot(activations, modulation_weight, preferred_element_type=jnp.float32)
    summed = of_everyone(partial_value, SP)
    modulation = gather_directly(summed, TP, 1)
    hidden = modulated(
        latent, norm_gain, modulation[0, :model_width], modulation[0, model_width : 2 * model_width]
    )
    ctx_hidden = modulated(
        context,
        norm_gain,
        modulation[1, :model_width],
        modulation[1, model_width : 2 * model_width],
    )
    gate = modulation[0, 2 * model_width :]
    row_count = latent.shape[0]
    row_start = lax.axis_index(SP_TP) * row_count
    total_rows = row_count * lax.axis_size(SP_TP)
    positions = row_start + jnp.arange(row_count, dtype=jnp.int32)
    queries = (
        rotary(
            head_norm(
                jnp.dot(hidden, query_weight, preferred_element_type=jnp.float32), query_gain
            ),
            positions,
        )
        .astype(jnp.bfloat16)
        .reshape(row_count, query_width)
    )
    local_both = key_value_rows(hidden, positions, key_weight, value_weight, key_gain)
    band = padded(local_both, ((SP_TP, 1),), WINDOW)
    piece_rows = ctx_hidden.shape[0]
    projected = head_norm(
        jnp.dot(ctx_hidden, key_weight, preferred_element_type=jnp.float32), key_gain
    )
    projected = projected.astype(jnp.bfloat16).reshape(piece_rows, kv_width)
    value_rows = jnp.dot(ctx_hidden, value_weight, preferred_element_type=jnp.float32).astype(
        jnp.bfloat16
    )
    ctx_both = whole_of(
        jnp.concatenate([projected, value_rows], axis=1), (("sp_0", "sp_1"), ("tp_0", "tp_1")), 0
    )
    key_pos = row_start - WINDOW + jnp.arange(row_count + 2 * WINDOW, dtype=jnp.int32)
    allowed = (
        (jnp.abs(key_pos[None, :] - positions[:, None]) <= WINDOW)
        & (key_pos[None, :] >= 0)
        & (key_pos[None, :] < total_rows)
    )
    mixed = attend(
        queries,
        band[0],
        band[1],
        ctx_both[:, :kv_width],
        ctx_both[:, kv_width:],
        sink_logit,
        allowed,
        head_size,
    )
    update = jnp.dot(mixed, output_weight, preferred_element_type=jnp.float32)
    return (latent.astype(jnp.float32) + gate * update).astype(jnp.bfloat16)


def solution(mesh):
    torus = Mesh(mesh.devices.reshape(8, 4, 4, 2), ("sp_0", "sp_1", "tp_0", "tp_1"))
    in_specs = (
        P(SP_TP, None),
        P(SP_TP, None),
        P(SP),
        P(SP),
        P(SP, TP),
        P(),
        P(),
        P(),
        P(),
        P(),
        P(),
        P(),
        P(),
    )
    out_specs = P(SP_TP, None)
    return jax.shard_map(local, mesh=torus, in_specs=in_specs, out_specs=out_specs, check_vma=False)
```

profile of v0, /device:TPU:32, one launch (start us, length us, event | category | flops | bytes accessed | tf_op | source)
XLA Modules:
  0.0 111.2 jit_solution(15141489054610298491)
XLA Ops:
  1.9 11.2 %all-to-all-start = ((f32[32,2,768]{2,1,0:T(2,128)}), f32[32,2,768]{2,1,0:T(2,128)S(1)}, u32[]{:S(2)}, u32[]{:S(2)}) async-start(f32[32,2,768]{2,1,0:T(2,128)} %broadcast_in_dim.16), calls=%async_computation | async-start | bytes 393216 | tf_op jit(solution)/shard_map/all_to_all | solution.py:21
  13.8 1.7 %fusion.4 = f32[288]{0:T(512)S(1)} fusion(bf16[288,2048]{1,0:T(8,128)(2,1)} %param.13), kind=kLoop, calls=%fused_computation.11 | loop fusion | flops 1769184 | bytes 1180800 | tf_op jit(solution)/shard_map/reduce_sum | solution.py:67
  16.7 7.3 %all-to-all-done = f32[32,2,768]{2,1,0:T(2,128)S(1)} async-done(((f32[32,2,768]{2,1,0:T(2,128)}), f32[32,2,768]{2,1,0:T(2,128)S(1)}, u32[]{:S(2)}, u32[]{:S(2)}) %all-to-all-start) | async-done | bytes 196640 | tf_op jit(solution)/shard_map/all_to_all | solution.py:21
  24.7 4.5 %all-to-all-start.1 = ((f32[8,2,768]{2,1,0:T(2,128)}), f32[8,2,768]{2,1,0:T(2,128)S(1)}, u32[]{:S(2)}, u32[]{:S(2)}) async-start(f32[8,2,768]{2,1,0:T(2,128)} %broadcast_in_dim.17), calls=%async_computation.1 | async-start | bytes 98304 | tf_op jit(solution)/shard_map/all_to_all | solution.py:21
  30.6 4.1 %all-to-all-done.1 = f32[8,2,768]{2,1,0:T(2,128)S(1)} async-done(((f32[8,2,768]{2,1,0:T(2,128)}), f32[8,2,768]{2,1,0:T(2,128)S(1)}, u32[]{:S(2)}, u32[]{:S(2)}) %all-to-all-start.1) | async-done | bytes 49184 | tf_op jit(solution)/shard_map/all_to_all | solution.py:21
  34.7 1.5 %fusion.49 = f32[1,256]{1,0:T(1,128)S(1)} fusion(bf16[2048,256]{1,0:T(8,128)(2,1)} %param.20, f32[2,6144]{1,0:T(2,128)S(1)} %bitcast.126, f32[1,2048]{1,0:T(1,128)S(1)} %bitcast.140, bf16[1,2048]{1,0:T(2,128)(2,1)S(1)} %copy-done.14, f32[]{:T(128)S(6)} %rsqrt.44), kind=kOutput, calls=%fused_computation.107 | convolution fusion | flops 1062912 | bytes 1082372 | tf_op jit(solution)/shard_map/dot_general | solution.py:208
  40.4 1.5 %fusion.51 = f32[288,1024]{1,0:T(8,128)S(1)} fusion(bf16[2048,1024]{1,0:T(8,128)(2,1)S(1)} %copy-done.17, bf16[288,2048]{1,0:T(8,128)(2,1)S(1)} %copy-done.8, f32[2048]{0:T(1024)S(1)} %bitcast.131, f32[2048]{0:T(1024)S(1)} %bitcast.134, f32[2048]{0:T(1024)S(1)} %copy-done.19, f32[288]{0:T(512)S(1)} %add_rsqrt_fusion.2), kind=kOutput, calls=%fused_computation.108 | convolution fusion | flops 1211498496 | bytes 6579328 | tf_op jit(solution)/shard_map/dot_general | solution.py:197
  42.9 1.5 %reshape.338 = f32[288,2,4,128]{3,2,1,0:T(4,128)} reshape(f32[288,1024]{1,0:T(8,128)S(1)} %fusion.51) | data formatting | bytes 2359296 | tf_op jit(solution)/shard_map/reshape | solution.py:87
  44.5 1.7 %copy.97 = f32[288,1024]{0,1:T(8,128)S(1)} copy(f32[288,1024]{1,0:T(8,128)} %copy-done.2) | data formatting | bytes 2359296 | tf_op jit(solution)/shard_map/dot_general | solution.py:197
  48.5 4.5 %all-to-all-start.2 = ((bf16[32,2,256]{2,1,0:T(2,128)(2,1)}), bf16[32,2,256]{2,1,0:T(2,128)(2,1)S(1)}, u32[]{:S(2)}, u32[]{:S(2)}) async-start(bf16[32,2,256]{2,1,0:T(2,128)(2,1)} %reshape.355), calls=%async_computation.2 | async-start | bytes 65536 | tf_op jit(solution)/shard_map/all_to_all | solution.py:21
  58.2 1.9 %collective-permute-start = (bf16[2,128,256]{2,1,0:T(8,128)(2,1)}, bf16[2,128,256]{2,1,0:T(8,128)(2,1)}, u32[]{:S(2)}, u32[]{:S(2)}) collective-permute-start(bf16[2,128,256]{2,1,0:T(8,128)(2,1)} %get-tuple-element.11), channel_id=1, source_target_pairs={{0,1},{1,2},{2,3},{3,4},{4,5},{5,6},{6,7},{7,8},{8,9},{9,10},{10,1... | collective-permute-start | bytes 393224 | tf_op jit(solution)/shard_map/ppermute | solution.py:47
  60.2 8.0 %collective-permute-start.1 = (bf16[2,128,256]{2,1,0:T(8,128)(2,1)}, bf16[2,128,256]{2,1,0:T(8,128)(2,1)}, u32[]{:S(2)}, u32[]{:S(2)}) collective-permute-start(bf16[2,128,256]{2,1,0:T(8,128)(2,1)} %get-tuple-element.12), channel_id=1, source_target_pairs={{1,0},{2,1},{3,2},{4,3},{5,4},{6,5},{7,6},{8,7},{9,8},{10,9},{11,1... | collective-permute-start | bytes 393224 | tf_op jit(solution)/shard_map/ppermute | solution.py:48
  71.0 2.5 %copy.99 = f32[288,2,4,32]{3,0,2,1:T(8,128)} copy(f32[288,2,4,32]{0,3,2,1:T(8,128)} %bitcast.114) | data formatting | bytes 589824 | tf_op jit(solution)/shard_map/concatenate | solution.py:82
  74.9 1.4 %copy.100 = f32[288,2,4,32]{3,0,2,1:T(8,128)} copy(f32[288,2,4,32]{0,3,2,1:T(8,128)S(1)} %bitcast.112) | data formatting | bytes 589824 | tf_op jit(solution)/shard_map/concatenate | solution.py:82
  76.3 3.7 %fusion.14 = bf16[288,2,4,128]{3,0,2,1:T(8,128)(2,1)S(1)} fusion(f32[288,2,4,32]{3,0,2,1:T(8,128)} %copy.102, f32[288,2,4,32]{3,0,2,1:T(8,128)} %copy.101, f32[288,2,4,32]{3,0,2,1:T(8,128)} %copy.100, f32[288,2,4,32]{3,0,2,1:T(8,128)} %copy.99, f32[288,2,4,128]{3,2,1,0:T(4,128)S(1)} %copy-done.1, f32[288,128]{1,0:T(8,128)} %copy-done.3, ...), kind=kLoop, calls=%fused_computation.28 | loop fusion | flops 2654208 | bytes 3253760 | tf_op jit(solution)/shard_map/convert_element_type | solution.py:201
  80.8 3.4 %all-to-all-start.3 = ((bf16[8,32,1,512]{3,1,2,0:T(8,128)(2,1)}), bf16[8,32,1,512]{3,1,2,0:T(8,128)(2,1)S(1)}, u32[]{:S(2)}, u32[]{:S(2)}) async-start(bf16[8,32,1,512]{3,1,2,0:T(8,128)(2,1)} %broadcast_in_dim.22), calls=%async_computation.3 | async-start | bytes 524288 | tf_op jit(solution)/shard_map/all_to_all | solution.py:21
  86.2 3.9 %fusion.1 = (f32[2,4,288]{2,1,0:T(4,128)S(1)}, f32[2,544,288,4]{1,2,3,0:T(8,128)}) fusion(pred[288,544]{1,0:T(8,128)(4,1)S(1)} %fusion.19, bf16[288,2,4,128]{3,0,2,1:T(8,128)(2,1)S(1)} %fusion.14, bf16[544,2,128,1]{2,1,0,3:T(2,128)(2,1)S(1)} %bitcast.119), kind=kOutput, calls=%fused_computation.4 | convolution fusion | flops 324622080 | bytes 6047744 | tf_op jit(solution)/shard_map/rhgd,khd->hgrk/dot_general | solution.py:126
  90.1 1.6 %all-to-all-done.3 = bf16[8,32,1,512]{3,1,2,0:T(8,128)(2,1)S(1)} async-done(((bf16[8,32,1,512]{3,1,2,0:T(8,128)(2,1)}), bf16[8,32,1,512]{3,1,2,0:T(8,128)(2,1)S(1)}, u32[]{:S(2)}, u32[]{:S(2)}) %all-to-all-start.3) | async-done | bytes 262176 | tf_op jit(solution)/shard_map/all_to_all | solution.py:21
  92.5 1.7 %copy.108 = bf16[256,256]{0,1:T(8,128)(2,1)} copy(bf16[256,256]{1,0:T(8,128)(2,1)} %get-tuple-element.19) | data formatting | bytes 262144 | tf_op jit(solution)/shard_map/slice | solution.py:228
  94.2 1.7 %copy.105 = bf16[256,256]{0,1:T(8,128)(2,1)} copy(bf16[256,256]{1,0:T(8,128)(2,1)} %get-tuple-element.20) | data formatting | bytes 262144 | tf_op jit(solution)/shard_map/slice | solution.py:227
  95.8 1.6 %bitcast_reduce_fusion = (f32[2,4,288]{2,1,0:T(4,128)S(1)}, f32[2,256,288,4]{1,2,3,0:T(8,128)S(1)}) fusion(bf16[256,2,128,1]{0,2,3,1:T(8,128)(2,1)} %bitcast.121, bf16[288,2,4,128]{3,0,2,1:T(8,128)(2,1)S(1)} %fusion.14), kind=kOutput, calls=%fused_computation.17 | convolution fusion | flops 152172288 | bytes 3089408 | tf_op jit(solution)/shard_map/rhgd,khd->hgrk/dot_general | solution.py:131
  98.4 4.0 %fusion = f32[2,4,288]{2,1,0:T(4,128)S(1)} fusion(f32[2,544,288,4]{1,2,3,0:T(8,128)} %get-tuple-element.27, f32[2,4,288]{2,1,0:T(4,128)S(1)} %maximum_maximum_fusion, pred[288,544]{1,0:T(8,128)(4,1)S(1)} %fusion.19), kind=kLoop, calls=%fused_computation.3 | loop fusion | flops 5011200 | bytes 5188608 | tf_op jit(solution)/shard_map/reduce_sum | solution.py:145
  102.5 1.7 %fusion.2 = f32[2,128,4,288]{1,3,2,0:T(8,128)S(1)} fusion(f32[2,544,288,4]{1,2,3,0:T(8,128)S(1)} %bitcast.111, f32[2,4,288]{2,1,0:T(4,128)S(1)} %exponential_add_fusion, f32[2,4,288]{2,1,0:T(4,128)S(1)} %maximum_maximum_fusion, pred[288,544]{1,0:T(8,128)(4,1)S(1)} %fusion.19, bf16[544,2,128,1]{2,1,0,3:T(2,128)(2,1)S(1)} %bitcast.122), kind=kOutput, calls=%fused_computation.8 | convolution fusion | flops 327131136 | bytes 6646784 | tf_op jit(solution)/shard_map/hgrk,khd->rhgd/dot_general | solution.py:151
  106.6 4.6 %fusion.3 = bf16[288,2048]{1,0:T(8,128)(2,1)} fusion(bf16[288,1024]{1,0:T(8,128)(2,1)S(1)} %reshape.343, bf16[1024,2048]{1,0:T(8,128)(2,1)} %param.22, bf16[288,2048]{1,0:T(8,128)(2,1)S(1)} %copy-done.9, f32[2048]{0:T(1024)S(1)} %bitcast.128), kind=kOutput, calls=%fused_computation.10 | convolution fusion | flops 1210318848 | bytes 7151616 | tf_op jit(solution)/shard_map/dot_general | solution.py:233
  (114 shorter events, 28.9 us)
Async XLA Ops:
  0.0 36.2 %copy-start = (bf16[2048,256]{1,0:T(8,128)(2,1)S(1)}, bf16[2048,256]{1,0:T(8,128)(2,1)}, u32[]{:S(2)}) copy-start(bf16[2048,256]{1,0:T(8,128)(2,1)} %param.21) | copy-start | bytes 3145732
  0.0 29.2 %copy-start.14 = (bf16[1,2048]{1,0:T(2,128)(2,1)S(1)}, bf16[1,2048]{1,0:T(2,128)(2,1)}, u32[]{:S(2)}) copy-start(bf16[1,2048]{1,0:T(2,128)(2,1)} %param.14) | copy-start | bytes 12292
  0.0 30.5 %copy-start.20 = (f32[8]{0:T(128)S(1)}, f32[8]{0:T(128)}, u32[]{:S(2)}) copy-start(f32[8]{0:T(128)} %param.25) | copy-start | bytes 100
  0.0 34.7 %copy-start.19 = (f32[2048]{0:T(1024)S(1)}, f32[2048]{0:T(1024)}, u32[]{:S(2)}) copy-start(f32[2048]{0:T(1024)} %param.18) | copy-start | bytes 24580
  1.9 22.1 %all-to-all-start = ((f32[32,2,768]{2,1,0:T(2,128)}), f32[32,2,768]{2,1,0:T(2,128)S(1)}, u32[]{:S(2)}, u32[]{:S(2)}) async-start(f32[32,2,768]{2,1,0:T(2,128)} %broadcast_in_dim.16), calls=%async_computation | async-start | bytes 393216 | tf_op jit(solution)/shard_map/all_to_all | solution.py:21
  13.8 22.6 %copy-start.7 = (bf16[288,2048]{1,0:T(8,128)(2,1)S(1)}, bf16[288,2048]{1,0:T(8,128)(2,1)}, u32[]{:S(2)}) copy-start(bf16[288,2048]{1,0:T(8,128)(2,1)} %param.13) | copy-start | bytes 3538948
  16.3 39.6 %copy-start.3 = (f32[288,128]{1,0:T(8,128)}, f32[288,128]{1,0:T(8,128)S(1)}, u32[]{:S(2)}) copy-start(f32[288,128]{1,0:T(8,128)S(1)} %get-tuple-element.18) | copy-start | bytes 442372
  16.3 40.9 %copy-start.6 = (f32[288,128]{1,0:T(8,128)}, f32[288,128]{1,0:T(8,128)S(1)}, u32[]{:S(2)}) copy-start(f32[288,128]{1,0:T(8,128)S(1)} %get-tuple-element.17) | copy-start | bytes 442372
  24.7 10.0 %all-to-all-start.1 = ((f32[8,2,768]{2,1,0:T(2,128)}), f32[8,2,768]{2,1,0:T(2,128)S(1)}, u32[]{:S(2)}, u32[]{:S(2)}) async-start(f32[8,2,768]{2,1,0:T(2,128)} %broadcast_in_dim.17), calls=%async_computation.1 | async-start | bytes 98304 | tf_op jit(solution)/shard_map/all_to_all | solution.py:21
  37.8 2.7 %copy-start.17 = (bf16[2048,1024]{1,0:T(8,128)(2,1)S(1)}, bf16[2048,1024]{1,0:T(8,128)(2,1)}, u32[]{:S(2)}) copy-start(bf16[2048,1024]{1,0:T(8,128)(2,1)} %param.19) | copy-start | bytes 12582916
  42.9 3.5 %copy-start.15 = (f32[128]{0:T(128)S(1)}, f32[128]{0:T(128)}, u32[]{:S(2)}) copy-start(f32[128]{0:T(128)} %param.24) | copy-start | bytes 1540
  48.5 31.5 %all-to-all-start.2 = ((bf16[32,2,256]{2,1,0:T(2,128)(2,1)}), bf16[32,2,256]{2,1,0:T(2,128)(2,1)S(1)}, u32[]{:S(2)}, u32[]{:S(2)}) async-start(bf16[32,2,256]{2,1,0:T(2,128)(2,1)} %reshape.355), calls=%async_computation.2 | async-start | bytes 65536 | tf_op jit(solution)/shard_map/all_to_all | solution.py:21
  54.9 2.5 %copy-start.10 = (f32[288,256]{1,0:T(8,128)S(1)}, f32[288,256]{1,0:T(8,128)}, u32[]{:S(2)}) copy-start(f32[288,256]{1,0:T(8,128)} %fusion.54) | copy-start | bytes 884740
  56.9 11.5 %copy-start.16 = (f32[128]{0:T(128)S(1)}, f32[128]{0:T(128)}, u32[]{:S(2)}) copy-start(f32[128]{0:T(128)} %param.23) | copy-start | bytes 1540
  57.5 11.2 %copy-start.4 = (bf16[1,288,256]{2,1,0:T(8,128)(2,1)}, bf16[1,288,256]{2,1,0:T(8,128)(2,1)S(1)}, u32[]{:S(2)}) copy-start(bf16[1,288,256]{2,1,0:T(8,128)(2,1)S(1)} %fusion.25) | copy-start | bytes 442372
  58.2 26.0 %collective-permute-start = (bf16[2,128,256]{2,1,0:T(8,128)(2,1)}, bf16[2,128,256]{2,1,0:T(8,128)(2,1)}, u32[]{:S(2)}, u32[]{:S(2)}) collective-permute-start(bf16[2,128,256]{2,1,0:T(8,128)(2,1)} %get-tuple-element.11), channel_id=1, source_target_pairs={{0,1},{1,2},{2,3},{3,4},{4,5},{5,6},{6,7},{7,8},{8,9},{9,10},{10,1... | collective-permute-start | bytes 393224 | tf_op jit(solution)/shard_map/ppermute | solution.py:47
  60.2 24.0 %collective-permute-start.1 = (bf16[2,128,256]{2,1,0:T(8,128)(2,1)}, bf16[2,128,256]{2,1,0:T(8,128)(2,1)}, u32[]{:S(2)}, u32[]{:S(2)}) collective-permute-start(bf16[2,128,256]{2,1,0:T(8,128)(2,1)} %get-tuple-element.12), channel_id=1, source_target_pairs={{1,0},{2,1},{3,2},{4,3},{5,4},{6,5},{7,6},{8,7},{9,8},{10,9},{11,1... | collective-permute-start | bytes 393224 | tf_op jit(solution)/shard_map/ppermute | solution.py:48
  71.0 5.3 %copy-start.1 = (f32[288,2,4,128]{3,2,1,0:T(4,128)S(1)}, f32[288,2,4,128]{3,2,1,0:T(4,128)}, u32[]{:S(2)}) copy-start(f32[288,2,4,128]{3,2,1,0:T(4,128)} %reshape.338) | copy-start | bytes 3538948
  76.3 7.9 %copy-start.5 = (bf16[1,288,256]{2,1,0:T(8,128)(2,1)S(1)}, bf16[1,288,256]{2,1,0:T(8,128)(2,1)}, u32[]{:S(2)}) copy-start(bf16[1,288,256]{2,1,0:T(8,128)(2,1)} %copy-done.4) | copy-start | bytes 442372
  80.8 10.8 %all-to-all-start.3 = ((bf16[8,32,1,512]{3,1,2,0:T(8,128)(2,1)}), bf16[8,32,1,512]{3,1,2,0:T(8,128)(2,1)S(1)}, u32[]{:S(2)}, u32[]{:S(2)}) async-start(bf16[8,32,1,512]{3,1,2,0:T(8,128)(2,1)} %broadcast_in_dim.22), calls=%async_computation.3 | async-start | bytes 524288 | tf_op jit(solution)/shard_map/all_to_all | solution.py:21
  91.8 10.7 %slice-start = ((s8[5898240]{0:T(1024)(128)(4,1)}), s8[1703936]{0:T(1024)(128)(4,1)S(1)}, s32[]{:S(2)}) async-start(s8[5898240]{0:T(1024)(128)(4,1)} %bitcast.110), calls=%async_computation.4 | async-start | bytes 3407872
  97.5 5.0 %slice-start.1 = ((s8[5898240]{0:T(1024)(128)(4,1)}), s8[4194304]{0:T(1024)(128)(4,1)S(1)}, s32[]{:S(2)}) async-start(s8[5898240]{0:T(1024)(128)(4,1)} %bitcast.110), calls=%async_computation.5 | async-start | bytes 8388608
  98.4 4.1 %copy-start.12 = (bf16[544,2,128]{2,1,0:T(2,128)(2,1)S(1)}, bf16[544,2,128]{2,1,0:T(2,128)(2,1)}, u32[]{:S(2)}) copy-start(bf16[544,2,128]{2,1,0:T(2,128)(2,1)} %reshape_squeeze.6) | copy-start | bytes 835588
  102.5 1.7 %copy-start.13 = (bf16[256,256]{0,1:T(8,128)(2,1)S(1)}, bf16[256,256]{0,1:T(8,128)(2,1)}, u32[]{:S(2)}) copy-start(bf16[256,256]{0,1:T(8,128)(2,1)} %copy.108) | copy-start | bytes 393220
  (5 other events, 6.6 us)
where the time goes:
time: 112 us; the launch traced here: 111 us
  starting transfers between devices  33.5 us (30%)
  local copies, waits for them, and re-layouts  24.4 us (22%)
  matrix products  19.8 us (18%)
  other arithmetic  19.2 us (17%)
  waiting for transfers between devices  13 us (12%)
  between operations  1.24 us (1%)
    all_to_all x4, starting transfers between devices, copy_for_each(): return lax.all_to_all(copies, axis, split_axis=0, concat_axis=0, tiled=True)  23.6 us
    all_to_all x4, waiting for transfers between devices, copy_for_each(): return lax.all_to_all(copies, axis, split_axis=0, concat_axis=0, tiled=True)  13 us
    ppermute x1, starting transfers between devices, padded(): lax.ppermute(first, axis, [(b, a) for a, b in up])  8.04 us
    concatenate x4, local copies, waits for them, and re-layouts, rotary(): jnp.concatenate([turn_halves(row_half), turn_halves(col_half)], axis=-1)  6.7 us
    dot_general x1, matrix products, local(): update = jnp.dot(mixed, output_weight, preferred_element_type=jnp.float32)  4.62 us
    reduce_sum x1, other arithmetic, attend(): jnp.sum(near_exp, axis=-1, keepdims=True)  3.98 us
    dot_general x1, matrix products, attend(): jnp.einsum('rhgd,khd->hgrk', grouped, near_keys, preferred_element_type=j...  3.85 us
    convert_element_type x1, other arithmetic, local(): queries = rotary(head_norm(jnp.dot(hidden, query_weight, preferred_elemen...  3.71 us
  transfers between devices with their start and end apart: 6, of which 3 were waited for; matrix products, arithmetic and copies ran while one was open for 25% of the time, Pallas kernels for 0%

commit v1 on v0

v1 whole, which is shorter than its diff:
```python
import functools

import jax
import jax.numpy as jnp
from jax import lax
from jax.experimental import pallas as pl
from jax.experimental.pallas import tpu as pltpu
from jax.sharding import Mesh
from jax.sharding import PartitionSpec as P

WINDOW = 128
GRID_W = 64
HEAD = 128
HEADS = 8
KV_HEADS = 2
GROUP = HEADS // KV_HEADS
CHUNK = 96
EPS = 1e-06
ROPE_BASE = 10000.0
FAR_LOGIT = -1e30
LOG2E = 1.4426950408889634
MIB = 1024 * 1024
ALL_VMEM = 67_043_328
GROUP_ROWS = 32

AXES = ("z", "x", "y", "c")
FIRST = ("z", "c")
SECOND = ("x", "y")

F32 = jnp.float32
BF16 = jnp.bfloat16


def rms_scale(v):
    return lax.rsqrt(jnp.mean(v * v, axis=-1, keepdims=True) + EPS)


def high_low(v):
    high = v.astype(BF16).astype(F32)
    return high, v - high


def exchange(array, axes):
    return lax.all_to_all(array, axes, split_axis=0, concat_axis=0, tiled=True)


def copy_all(pairs, sems):
    copies = [
        pltpu.make_async_copy(src, dst, sems.at[i]) for i, (src, dst) in enumerate(pairs)
    ]
    for copy in copies:
        copy.start()
    return copies


def partial_kernel(
    cond_hbm, cctx_hbm, weight_hbm, ctx_hbm, out_ref,
    cond_ref, cctx_ref, weight_ref, ctx_ref, act_ref, rows_ref, sems,
):
    copies = copy_all(
        [(cond_hbm, cond_ref), (cctx_hbm, cctx_ref), (weight_hbm, weight_ref), (ctx_hbm, ctx_ref)],
        sems,
    )
    width = weight_ref.shape[1]
    model = ctx_ref.shape[1]
    act_ref[...] = jnp.zeros_like(act_ref)
    rows_ref[...] = jnp.zeros_like(rows_ref)
    for copy in copies:
        copy.wait()
    act_ref[0:1, :] = jax.nn.silu(cond_ref[...])
    act_ref[1:2, :] = jax.nn.silu(cctx_ref[...])
    part = jnp.dot(act_ref[...].astype(BF16), weight_ref[...], preferred_element_type=F32)
    high, low = high_low(part)
    rows_ref[0:2, :] = high[0:2]
    rows_ref[2:4, :] = low[0:2]
    ctx = ctx_ref[...].astype(F32)
    for i in range(3):
        size = min(width, model - i * width)
        rows_ref[4 + i : 5 + i, 0:size] = ctx[:, i * width : i * width + size]
    packed = rows_ref[...].astype(BF16)
    for i in range(out_ref.shape[0]):
        out_ref[i] = packed


def edges_kernel(lat_hbm, low_ref, high_ref, sems):
    own = lat_hbm.shape[0]
    copies = copy_all(
        [
            (lat_hbm.at[pl.ds(0, WINDOW)], low_ref),
            (lat_hbm.at[pl.ds(own - WINDOW, WINDOW)], high_ref),
        ],
        sems,
    )
    for copy in copies:
        copy.wait()


def middle_kernel(in_ref, out_ref, ctx_out, rows_ref, ctx_ref):
    members, _, width = in_ref.shape
    model = ctx_out.shape[1]
    for c in range(2):
        total = None
        for z in range(members // 2):
            m = 2 * z + c
            rows = in_ref[m].astype(F32)
            total = rows if total is None else total + rows
            for i in range(3):
                size = min(width, model - i * width)
                ctx_ref[m : m + 1, i * width : i * width + size] = rows[4 + i : 5 + i, 0:size]
        rows_ref[0:8, :] = total
        high, low = high_low(rows_ref[0:2, :] + rows_ref[2:4, :])
        rows_ref[8 + 4 * c : 10 + 4 * c, :] = high
        rows_ref[10 + 4 * c : 12 + 4 * c, :] = low
    packed = rows_ref[8:16, :].astype(BF16)
    for i in range(out_ref.shape[0]):
        out_ref[i] = packed
    ctx_out[...] = ctx_ref[...].astype(BF16)


def context_kernel(
    second_ref, c0_ref, c1_ref, c2_ref, c3_ref, gain_ref, wk_ref, wv_ref, kgain_ref,
    kv_out, vec_out, mod_ref, tmp_ref, hid_ref,
):
    members, _, width = second_ref.shape
    model = gain_ref.shape[1]
    side = 4
    for y in range(side):
        total = second_ref[y].astype(F32)
        for x in range(1, members // side):
            total += second_ref[x * side + y].astype(F32)
        tmp_ref[...] = total
        for c in range(2):
            at = (2 * y + c) * width
            mod_ref[0:2, at : at + width] = (
                tmp_ref[4 * c : 4 * c + 2, :] + tmp_ref[4 * c + 2 : 4 * c + 4, :]
            )
    gain = gain_ref[...]
    vec_out[0:1, :] = gain * (1.0 + mod_ref[0:1, model : 2 * model])
    vec_out[1:2, :] = mod_ref[0:1, 0:model]
    vec_out[2:3, :] = mod_ref[0:1, 2 * model : 3 * model]
    scale = gain * (1.0 + mod_ref[1:2, model : 2 * model])
    shift = mod_ref[1:2, 0:model]
    for i, ref in enumerate((c0_ref, c1_ref, c2_ref, c3_ref)):
        rows = ref[...].astype(F32)
        n = rows.shape[0]
        hid_ref[i * n : (i + 1) * n, :] = (rows * rms_scale(rows) * scale + shift).astype(BF16)
    keys = jnp.dot(hid_ref[...], wk_ref[...], preferred_element_type=F32)
    kv_out[:, KV_HEADS * HEAD :] = jnp.dot(
        hid_ref[...], wv_ref[...], preferred_element_type=F32
    ).astype(BF16)
    for h in range(KV_HEADS):
        k = keys[:, h * HEAD : (h + 1) * HEAD]
        kv_out[:, h * HEAD : (h + 1) * HEAD] = (k * rms_scale(k) * kgain_ref[...]).astype(BF16)


def turn(v, table_ref, first, group, groups):
    turned = jnp.where(first, pltpu.roll(v, HEAD - 32, 1), pltpu.roll(v, 32, 1))
    parts = []
    for i in range(groups):
        rows = slice(i * GROUP_ROWS, (i + 1) * GROUP_ROWS)
        at = pl.ds((group + i) * GROUP_ROWS, GROUP_ROWS)
        parts.append((v[rows] * table_ref[0, at, :] + turned[rows] * table_ref[1, at, :]).astype(BF16))
    return jnp.concatenate(parts, axis=0)


def project_kernel(
    start_ref, low_ref, mid_ref, high_ref, vec_ref, wk_ref, wv_ref, qgain_ref, kgain_ref,
    row_ref, col_ref, wq_hbm,
    q_out, k_out, v_out, hid_ref, table_ref, wq_ref, sem,
):
    load = pltpu.make_async_copy(wq_hbm, wq_ref, sem)
    load.start()
    own = mid_ref.shape[0]
    rows = own + 2 * WINDOW
    scale = vec_ref[0:1, :]
    shift = vec_ref[1:2, :]
    at = 0
    for ref in (low_ref, mid_ref, high_ref):
        for r in range(0, ref.shape[0], 32):
            v = ref[r : r + 32, :].astype(F32)
            hid_ref[at : at + 32, :] = (v * rms_scale(v) * scale + shift).astype(BF16)
            at += 32
    block = start_ref[0] // GROUP_ROWS - WINDOW // GROUP_ROWS
    first_row = lax.shift_right_arithmetic(block, 1)
    for i in range(rows // GROUP_ROWS):
        row = lax.shift_right_arithmetic(block + i, 1) - first_row
        half = lax.bitwise_and(block + i, 1) * GROUP_ROWS
        for t in range(2):
            table_ref[t, i * GROUP_ROWS : (i + 1) * GROUP_ROWS, :] = (
                row_ref[t, pl.ds(row, 1), :] + col_ref[t, pl.ds(half, GROUP_ROWS), :]
            )
    lane = lax.broadcasted_iota(jnp.int32, (1, HEAD), 1)
    first = (lane % 64) < 32
    v_out[...] = jnp.dot(hid_ref[...], wv_ref[...], preferred_element_type=F32).astype(BF16)
    keys = jnp.dot(hid_ref[...], wk_ref[...], preferred_element_type=F32)
    kgain = kgain_ref[...]
    for h in range(KV_HEADS):
        k = keys[:, h * HEAD : (h + 1) * HEAD]
        k = k * rms_scale(k) * kgain
        k_out[:, h * HEAD : (h + 1) * HEAD] = turn(k, table_ref, first, 0, rows // GROUP_ROWS)
    qgain = qgain_ref[...]
    load.wait()
    for pair in range(HEADS // 2):
        at = pair * 2 * HEAD
        both = jnp.dot(
            hid_ref[WINDOW : WINDOW + own, :], wq_ref[:, at : at + 2 * HEAD],
            preferred_element_type=F32,
        )
        for h in range(2):
            q = both[:, h * HEAD : (h + 1) * HEAD]
            q = q * rms_scale(q) * qgain
            q = turn(q, table_ref, first, WINDOW // GROUP_ROWS, own // GROUP_ROWS)
            for c in range(own // CHUNK):
                q_out[c, 2 * pair + h] = q[c * CHUNK : (c + 1) * CHUNK]


def attend_kernel(
    start_ref, sink_ref, q_ref, k_ref, v_ref, x0_ref, x1_ref, x2_ref, x3_ref, lat_ref, vec_ref,
    wo_hbm, out_ref, mix_ref, vals_ref, ctx_ref, wo_ref, sem, *, total_rows,
):
    load = pltpu.make_async_copy(wo_hbm, wo_ref, sem)
    load.start()
    chunks = q_ref.shape[0]
    rows = k_ref.shape[0]
    far = ctx_ref.shape[0]
    for i, ref in enumerate((x0_ref, x1_ref, x2_ref, x3_ref)):
        n = ref.shape[0]
        ctx_ref[i * n : (i + 1) * n, :] = ref[...]
    width = CHUNK + 2 * WINDOW
    factor = HEAD ** (-0.5) * LOG2E
    kv = KV_HEADS * HEAD
    for g in range(KV_HEADS):
        vals_ref[g, 0:rows, 0:HEAD] = v_ref[:, g * HEAD : (g + 1) * HEAD]
        vals_ref[g, rows : rows + far, 0:HEAD] = ctx_ref[:, kv + g * HEAD : kv + (g + 1) * HEAD]
        vals_ref[g, :, HEAD:] = jnp.ones_like(vals_ref[g, :, HEAD:])
    row = lax.broadcasted_iota(jnp.int32, (CHUNK, width), 0)
    col = lax.broadcasted_iota(jnp.int32, (CHUNK, width), 1)
    nt = (((1,), (1,)), ((), ()))
    for c in range(chunks):
        pos = start_ref[0] - WINDOW + c * CHUNK + col
        allowed = (col >= row) & (col <= row + 2 * WINDOW) & (pos >= 0) & (pos < total_rows)
        bias = jnp.where(allowed, 0.0, FAR_LOGIT)
        for g in range(KV_HEADS):
            q = q_ref[c, g * GROUP : (g + 1) * GROUP].reshape(GROUP * CHUNK, HEAD)
            k = k_ref[c * CHUNK : c * CHUNK + width, g * HEAD : (g + 1) * HEAD]
            near = lax.dot_general(q, k, nt, preferred_element_type=F32)
            near = near.reshape(GROUP, CHUNK, width) + bias[None]
            ctx = lax.dot_general(
                q, ctx_ref[:, g * HEAD : (g + 1) * HEAD], nt, preferred_element_type=F32
            ).reshape(GROUP, CHUNK, far)
            sink = jnp.concatenate(
                [jnp.full((1, CHUNK, 1), sink_ref[g * GROUP + h], F32) for h in range(GROUP)], axis=0
            ) * (HEAD**0.5)
            top = jnp.maximum(
                jnp.maximum(
                    jnp.max(near, axis=-1, keepdims=True), jnp.max(ctx, axis=-1, keepdims=True)
                ),
                sink,
            )
            near = jnp.exp2((near - top) * factor).astype(BF16).reshape(GROUP * CHUNK, width)
            ctx = jnp.exp2((ctx - top) * factor).astype(BF16).reshape(GROUP * CHUNK, far)
            tail = jnp.exp2((sink - top) * factor).reshape(GROUP * CHUNK, 1)
            mixed = jnp.dot(
                near, vals_ref[g, c * CHUNK : c * CHUNK + width, :], preferred_element_type=F32
            ) + jnp.dot(ctx, vals_ref[g, rows : rows + far, :], preferred_element_type=F32)
            mixed = (mixed[:, :HEAD] / (mixed[:, HEAD:] + tail)).astype(BF16)
            for h in range(GROUP):
                at = (g * GROUP + h) * HEAD
                mix_ref[c * CHUNK : (c + 1) * CHUNK, at : at + HEAD] = mixed[
                    h * CHUNK : (h + 1) * CHUNK
                ]
    model = out_ref.shape[1]
    load.wait()
    for at in range(0, model, 256):
        update = jnp.dot(mix_ref[...], wo_ref[:, at : at + 256], preferred_element_type=F32)
        out_ref[:, at : at + 256] = (
            lat_ref[:, at : at + 256].astype(F32) + vec_ref[2:3, at : at + 256] * update
        ).astype(BF16)


def call(kernel, outs, scratch, limit, flops, *args, smem=0, hbm=()):
    vmem = pl.BlockSpec(memory_space=pltpu.VMEM)
    many = isinstance(outs, (list, tuple))
    specs = [pl.BlockSpec(memory_space=pltpu.SMEM)] * smem + [vmem] * (len(args) - smem)
    for i in hbm:
        specs[i] = pl.BlockSpec(memory_space=pltpu.HBM)
    return pl.pallas_call(
        kernel,
        out_shape=outs,
        in_specs=specs,
        out_specs=[vmem] * len(outs) if many else vmem,
        scratch_shapes=scratch,
        compiler_params=pltpu.CompilerParams(vmem_limit_bytes=limit),
        cost_estimate=pl.CostEstimate(flops=flops, bytes_accessed=flops // 256, transcendentals=0),
    )(*args)


def rotary_tables(first_row, rows):
    quarter = HEAD // 4
    inverse = jnp.power(ROPE_BASE, -jnp.arange(quarter, dtype=F32) / quarter)
    sign = jnp.where(jnp.arange(HEAD // 2) < HEAD // 4, -1.0, 1.0)

    def table(positions):
        angles = positions.astype(F32)[:, None] * inverse
        angles = jnp.concatenate([angles, angles], axis=-1)
        return jnp.stack([jnp.cos(angles), jnp.sin(angles) * sign])

    by_rows = table(first_row + jnp.arange(rows, dtype=jnp.int32))
    by_cols = table(jnp.arange(GRID_W, dtype=jnp.int32))
    none = ((0, 0), (0, 0))
    return (
        jnp.pad(by_rows, (*none, (0, HEAD // 2))),
        jnp.pad(by_cols, (*none, (HEAD // 2, 0))),
    )


def spread(array, axis):
    size = lax.axis_size(axis)
    return [array] + [
        lax.ppermute(array, axis, [(i, (i + k) % size) for i in range(size)])
        for k in range(1, size)
    ]


def local(
    latent,
    context,
    condition,
    context_condition,
    modulation_weight,
    norm_gain,
    query_weight,
    key_weight,
    value_weight,
    output_weight,
    query_gain,
    key_gain,
    sink_logit,
):
    own, model = latent.shape
    width = modulation_weight.shape[1]
    kv = key_weight.shape[1]
    world = lax.axis_size(AXES)
    members = lax.axis_size(FIRST)
    start = lax.axis_index(AXES) * own
    total_rows = own * world
    up = [(i, i + 1) for i in range(world - 1)]
    down = [(i + 1, i) for i in range(world - 1)]
    struct = jax.ShapeDtypeStruct
    span = own + 2 * WINDOW
    start_ref = start.astype(jnp.int32)[None]

    payload = call(
        partial_kernel,
        struct((members, 8, width), BF16),
        [
            pltpu.VMEM((1, condition.shape[0]), F32),
            pltpu.VMEM((1, condition.shape[0]), F32),
            pltpu.VMEM(modulation_weight.shape, BF16),
            pltpu.VMEM((1, model), BF16),
            pltpu.VMEM((8, condition.shape[0]), F32),
            pltpu.VMEM((8, width), F32),
            pltpu.SemaphoreType.DMA((4,)),
        ],
        ALL_VMEM, 1000,
        condition[None], context_condition[None], modulation_weight, context,
        hbm=(0, 1, 2, 3),
    )
    with jax.named_scope("first"):
        first = exchange(payload, FIRST)
    with jax.named_scope("edges"):
        low, high = call(
            edges_kernel,
            [struct((WINDOW, model), BF16), struct((WINDOW, model), BF16)],
            [pltpu.SemaphoreType.DMA((2,))],
            ALL_VMEM, 1000,
            latent,
            hbm=(0,),
        )
    with jax.named_scope("halo"):
        below = lax.ppermute(high, AXES, up)
        above = lax.ppermute(low, AXES, down)
    by_rows, by_cols = rotary_tables(lax.div(start - WINDOW, GRID_W), 16)

    payload, ctx_rows = call(
        middle_kernel,
        [struct((lax.axis_size(SECOND), 8, width), BF16), struct((members, model), BF16)],
        [pltpu.VMEM((16, width), F32), pltpu.VMEM((members, model), F32)],
        4 * MIB, 1000,
        first,
    )
    with jax.named_scope("second"):
        second = exchange(payload, SECOND)
    with jax.named_scope("rows"):
        ctx_parts = spread(ctx_rows, "x")
    ctx_kv, vectors = call(
        context_kernel,
        [struct((4 * members, 2 * kv), BF16), struct((8, model), F32)],
        [
            pltpu.VMEM((8, 3 * model), F32),
            pltpu.VMEM((8, width), F32),
            pltpu.VMEM((4 * members, model), BF16),
        ],
        8 * MIB, 4_000_000_000,
        second, *ctx_parts, norm_gain[None], key_weight, value_weight, key_gain[None],
    )
    with jax.named_scope("pairs"):
        ctx_all = spread(ctx_kv, "y")
    queries, keys, values = call(
        project_kernel,
        [
            struct((own // CHUNK, HEADS, CHUNK, HEAD), BF16),
            struct((span, kv), BF16),
            struct((span, kv), BF16),
        ],
        [
            pltpu.VMEM((span, model), BF16),
            pltpu.VMEM((2, span, HEAD), F32),
            pltpu.VMEM(query_weight.shape, BF16),
            pltpu.SemaphoreType.DMA,
        ],
        20 * MIB, 6_000_000_000,
        start_ref, below, latent, above, vectors, key_weight, value_weight,
        query_gain[None], key_gain[None], by_rows, by_cols, query_weight,
        smem=1, hbm=(11,),
    )
    return call(
        functools.partial(attend_kernel, total_rows=total_rows),
        struct((own, model), BF16),
        [
            pltpu.VMEM((own, HEADS * HEAD), BF16),
            pltpu.VMEM((KV_HEADS, span + world, 2 * HEAD), BF16),
            pltpu.VMEM((world, 2 * kv), BF16),
            pltpu.VMEM(output_weight.shape, BF16),
            pltpu.SemaphoreType.DMA,
        ],
        20 * MIB, 3_000_000_000,
        start_ref, sink_logit, queries, keys, values, *ctx_all, latent, vectors, output_weight,
        smem=2, hbm=(11,),
    )


def solution(mesh):
    torus = Mesh(mesh.devices.reshape(8, 4, 4, 2), AXES)
    rows = P(AXES, None)
    in_specs = (
        rows,
        rows,
        P(("z", "x")),
        P(("z", "x")),
        P(("z", "x"), ("y", "c")),
        P(),
        P(),
        P(),
        P(),
        P(),
        P(),
        P(),
        P(),
    )
    return jax.shard_map(local, mesh=torus, in_specs=in_specs, out_specs=rows, check_vma=False)
```

time: 112 us -> 61.3 us (0.55)
  the two profiles are of different devices: /device:TPU:32 before, /device:TPU:8 now
where the time goes in v1:
time: 61.3 us; the launch traced here: 60.8 us
  starting transfers between devices  30.8 us (50%)
  Pallas kernels  18.4 us (30%)
  waiting for transfers between devices  6.7 us (11%)
  local copies, waits for them, and re-layouts  3.84 us (6%)
    pallas_call x6, Pallas kernels, call(): pl.pallas_call(kernel, out_shape=outs, in_specs=specs, out_specs=[vmem] *...  18.4 us
    all_to_all x2, starting transfers between devices, exchange(): return lax.all_to_all(array, axes, split_axis=0, concat_axis=0, tiled=True)  16 us
    ppermute x6, starting transfers between devices, spread(): lax.ppermute(array, axis, [(i, (i + k) % size) for i in range(size)])  9.25 us
    ppermute x6, waiting for transfers between devices, spread(): lax.ppermute(array, axis, [(i, (i + k) % size) for i in range(size)])  5.08 us
    unnamed x24, local copies, waits for them, and re-layouts  3.84 us
    ppermute x1, starting transfers between devices, local(): above = lax.ppermute(low, AXES, down)  3.29 us
    ppermute x1, starting transfers between devices, local(): below = lax.ppermute(high, AXES, up)  2.27 us
    all_to_all x2, waiting for transfers between devices, exchange(): return lax.all_to_all(array, axes, split_axis=0, concat_axis=0, tiled=True)  1.61 us
  transfers between devices with their start and end apart: 10, of which 4 were waited for; matrix products, arithmetic and copies ran while one was open for 1% of the time, Pallas kernels for 16%

profile of v1, /device:TPU:8, one launch (start us, length us, event | category | flops | bytes accessed | tf_op | source)
XLA Modules:
  0.0 60.8 jit_solution(13384980929714485086)
XLA Ops:
  0.0 1.8 %shard_map.127 = bf16[16,8,768]{2,1,0:T(8,128)(2,1)} custom-call(f32[1,64]{1,0:T(1,128)} %bitcast.14, f32[1,64]{1,0:T(1,128)} %bitcast.15, bf16[64,768]{1,0:T(8,128)(2,1)} %weight_hbm.1, bf16[1,2048]{1,0:T(2,128)(2,1)} %ctx_hbm.1), custom_call_target="tpu_custom_call" | custom-call | flops 1000 | bytes 3 | tf_op jit(solution)/shard_map/pallas_call | solution.py:287
  1.8 8.6 %all-to-all-start = ((bf16[16,8,768]{2,1,0:T(8,128)(2,1)}), bf16[16,8,768]{2,1,0:T(8,128)(2,1)}, u32[]{:S(2)}, u32[]{:S(2)}) async-start(bf16[16,8,768]{2,1,0:T(8,128)(2,1)} %shard_map.127), calls=%async_computation | async-start | bytes 393216 | tf_op jit(solution)/shard_map/first/all_to_all | solution.py:44
  10.4 2.2 %edges.1 = (bf16[128,2048]{1,0:T(8,128)(2,1)}, bf16[128,2048]{1,0:T(8,128)(2,1)}) custom-call(bf16[288,2048]{1,0:T(8,128)(2,1)} %lat_ref.1), custom_call_target="tpu_custom_call" | custom-call | flops 1000 | bytes 3 | tf_op jit(solution)/shard_map/edges/pallas_call | solution.py:287
  12.6 2.3 %collective-permute-start = (bf16[128,2048]{1,0:T(8,128)(2,1)}, bf16[128,2048]{1,0:T(8,128)(2,1)S(1)}, u32[]{:S(2)}, u32[]{:S(2)}) collective-permute-start(bf16[128,2048]{1,0:T(8,128)(2,1)} %get-tuple-element.14), channel_id=1, source_target_pairs={{0,1},{1,2},{2,3},{3,4},{4,5},{5,6},{6,7},{7,8},{8,9},{9,10},{10,1... | collective-permute-start | bytes 1572872 | tf_op jit(solution)/shard_map/halo/ppermute | solution.py:381
  14.9 3.3 %collective-permute-start.1 = (bf16[128,2048]{1,0:T(8,128)(2,1)}, bf16[128,2048]{1,0:T(8,128)(2,1)S(1)}, u32[]{:S(2)}, u32[]{:S(2)}) collective-permute-start(bf16[128,2048]{1,0:T(8,128)(2,1)} %get-tuple-element.15), channel_id=1, source_target_pairs={{1,0},{2,1},{3,2},{4,3},{5,4},{6,5},{7,6},{8,7},{9,8},{10,9},{11,1... | collective-permute-start | bytes 1572872 | tf_op jit(solution)/shard_map/halo/ppermute | solution.py:382
  18.8 1.6 %all-to-all-done.in_ref = bf16[16,8,768]{2,1,0:T(8,128)(2,1)} async-done(((bf16[16,8,768]{2,1,0:T(8,128)(2,1)}), bf16[16,8,768]{2,1,0:T(8,128)(2,1)}, u32[]{:S(2)}, u32[]{:S(2)}) %all-to-all-start) | async-done | bytes 196640 | tf_op jit(solution)/shard_map/first/all_to_all | solution.py:44
  20.4 1.7 %shard_map.128 = (bf16[16,8,768]{2,1,0:T(8,128)(2,1)}, bf16[16,2048]{1,0:T(8,128)(2,1)S(1)}) custom-call(bf16[16,8,768]{2,1,0:T(8,128)(2,1)} %all-to-all-done.in_ref), custom_call_target="tpu_custom_call" | custom-call | flops 1000 | bytes 3 | tf_op jit(solution)/shard_map/pallas_call | solution.py:287
  22.1 7.4 %all-to-all-start.1 = ((bf16[16,8,768]{2,1,0:T(8,128)(2,1)}), bf16[16,8,768]{2,1,0:T(8,128)(2,1)S(1)}, u32[]{:S(2)}, u32[]{:S(2)}) async-start(bf16[16,8,768]{2,1,0:T(8,128)(2,1)} %get-tuple-element.16), calls=%async_computation.1 | async-start | bytes 393216 | tf_op jit(solution)/shard_map/second/all_to_all | solution.py:44
  29.6 2.8 %collective-permute-start.4 = (bf16[16,2048]{1,0:T(8,128)(2,1)S(1)}, bf16[16,2048]{1,0:T(8,128)(2,1)S(1)}, u32[]{:S(2)}, u32[]{:S(2)}) collective-permute-start(bf16[16,2048]{1,0:T(8,128)(2,1)S(1)} %get-tuple-element.17.c0_ref), channel_id=1, source_target_pairs={{0,24},{8,0},{16,8},{24,16},{1,25},{9,1},{17,9},{25,17},{2,26},{10... | collective-permute-start | bytes 196616 | tf_op jit(solution)/shard_map/rows/ppermute | solution.py:320
  32.3 0.9 %collective-permute-start.3 = (bf16[16,2048]{1,0:T(8,128)(2,1)S(1)}, bf16[16,2048]{1,0:T(8,128)(2,1)S(1)}, u32[]{:S(2)}, u32[]{:S(2)}) collective-permute-start(bf16[16,2048]{1,0:T(8,128)(2,1)S(1)} %get-tuple-element.17.c0_ref), channel_id=1, source_target_pairs={{0,16},{8,24},{16,0},{24,8},{1,17},{9,25},{17,1},{25,9},{2,18},{10... | collective-permute-start | bytes 196616 | tf_op jit(solution)/shard_map/rows/ppermute | solution.py:320
  33.2 0.9 %collective-permute-start.2 = (bf16[16,2048]{1,0:T(8,128)(2,1)S(1)}, bf16[16,2048]{1,0:T(8,128)(2,1)S(1)}, u32[]{:S(2)}, u32[]{:S(2)}) collective-permute-start(bf16[16,2048]{1,0:T(8,128)(2,1)S(1)} %get-tuple-element.17.c0_ref), channel_id=1, source_target_pairs={{0,8},{8,16},{16,24},{24,0},{1,9},{9,17},{17,25},{25,1},{2,10},{10... | collective-permute-start | bytes 196616 | tf_op jit(solution)/shard_map/rows/ppermute | solution.py:320
  34.0 2.1 %collective-permute-done.4.c3_ref = bf16[16,2048]{1,0:T(8,128)(2,1)S(1)} collective-permute-done((bf16[16,2048]{1,0:T(8,128)(2,1)S(1)}, bf16[16,2048]{1,0:T(8,128)(2,1)S(1)}, u32[]{:S(2)}, u32[]{:S(2)}) %collective-permute-start.4) | collective-permute-done | bytes 65568 | tf_op jit(solution)/shard_map/rows/ppermute | solution.py:320
  36.2 2.2 %collective-permute-done.3.c2_ref = bf16[16,2048]{1,0:T(8,128)(2,1)S(1)} collective-permute-done((bf16[16,2048]{1,0:T(8,128)(2,1)S(1)}, bf16[16,2048]{1,0:T(8,128)(2,1)S(1)}, u32[]{:S(2)}, u32[]{:S(2)}) %collective-permute-start.3) | collective-permute-done | bytes 65568 | tf_op jit(solution)/shard_map/rows/ppermute | solution.py:320
  38.4 0.7 %collective-permute-done.2.c1_ref = bf16[16,2048]{1,0:T(8,128)(2,1)S(1)} collective-permute-done((bf16[16,2048]{1,0:T(8,128)(2,1)S(1)}, bf16[16,2048]{1,0:T(8,128)(2,1)S(1)}, u32[]{:S(2)}, u32[]{:S(2)}) %collective-permute-start.2) | collective-permute-done | bytes 65568 | tf_op jit(solution)/shard_map/rows/ppermute | solution.py:320
  39.1 1.2 %copy-done.3 = bf16[2048,256]{1,0:T(8,128)(2,1)S(1)} copy-done((bf16[2048,256]{1,0:T(8,128)(2,1)S(1)}, bf16[2048,256]{1,0:T(8,128)(2,1)}, u32[]{:S(2)}) %copy-start.3) | copy-done | bytes 1048600
  40.4 1.2 %copy-done.5 = bf16[2048,256]{1,0:T(8,128)(2,1)S(1)} copy-done((bf16[2048,256]{1,0:T(8,128)(2,1)S(1)}, bf16[2048,256]{1,0:T(8,128)(2,1)}, u32[]{:S(2)}) %copy-start.5) | copy-done | bytes 1048600
  41.6 0.7 %copy-done.7 = f32[2048]{0:T(1024)S(1)} copy-done((f32[2048]{0:T(1024)S(1)}, f32[2048]{0:T(1024)}, u32[]{:S(2)}) %copy-start.7) | copy-done | bytes 8216
  42.3 0.7 %copy-done.8 = f32[128]{0:T(128)S(1)} copy-done((f32[128]{0:T(128)S(1)}, f32[128]{0:T(128)}, u32[]{:S(2)}) %copy-start.8) | copy-done | bytes 536
  43.0 0.7 %shard_map.129 = (bf16[64,512]{1,0:T(8,128)(2,1)S(1)}, f32[8,2048]{1,0:T(8,128)S(1)}) custom-call(bf16[16,8,768]{2,1,0:T(8,128)(2,1)S(1)} %all-to-all-done.1.second_ref, bf16[16,2048]{1,0:T(8,128)(2,1)S(1)} %get-tuple-element.17.c0_ref, bf16[16,2048]{1,0:T(8,128)(2,1)S(1)} %collective-permute-done.2.c1_ref, ...), custom_call_target="tpu_custom_call" | custom-call | flops 4000000000 | bytes 15625000 | tf_op jit(solution)/shard_map/pallas_call | solution.py:287
  43.7 0.6 %collective-permute-start.7 = (bf16[64,512]{1,0:T(8,128)(2,1)S(1)}, bf16[64,512]{1,0:T(8,128)(2,1)S(1)}, u32[]{:S(2)}, u32[]{:S(2)}) collective-permute-start(bf16[64,512]{1,0:T(8,128)(2,1)S(1)} %get-tuple-element.22.x0_ref), channel_id=1, source_target_pairs={{0,6},{2,0},{4,2},{6,4},{1,7},{3,1},{5,3},{7,5},{8,14},{10,8},{12,... | collective-permute-start | bytes 196616 | tf_op jit(solution)/shard_map/pairs/ppermute | solution.py:320
  44.3 2.4 %collective-permute-start.6 = (bf16[64,512]{1,0:T(8,128)(2,1)S(1)}, bf16[64,512]{1,0:T(8,128)(2,1)S(1)}, u32[]{:S(2)}, u32[]{:S(2)}) collective-permute-start(bf16[64,512]{1,0:T(8,128)(2,1)S(1)} %get-tuple-element.22.x0_ref), channel_id=1, source_target_pairs={{0,4},{2,6},{4,0},{6,2},{1,5},{3,7},{5,1},{7,3},{8,12},{10,14},{12... | collective-permute-start | bytes 196616 | tf_op jit(solution)/shard_map/pairs/ppermute | solution.py:320
  46.7 1.8 %collective-permute-start.5 = (bf16[64,512]{1,0:T(8,128)(2,1)S(1)}, bf16[64,512]{1,0:T(8,128)(2,1)S(1)}, u32[]{:S(2)}, u32[]{:S(2)}) collective-permute-start(bf16[64,512]{1,0:T(8,128)(2,1)S(1)} %get-tuple-element.22.x0_ref), channel_id=1, source_target_pairs={{0,2},{2,4},{4,6},{6,0},{1,3},{3,5},{5,7},{7,1},{8,10},{10,12},{12... | collective-permute-start | bytes 196616 | tf_op jit(solution)/shard_map/pairs/ppermute | solution.py:320
  48.5 4.9 %shard_map.130 = (bf16[3,8,96,128]{3,2,1,0:T(8,128)(2,1)S(1)}, bf16[544,256]{1,0:T(8,128)(2,1)S(1)}, bf16[544,256]{1,0:T(8,128)(2,1)S(1)}) custom-call(s32[1]{0:T(128)} %bitcast.start_ref, bf16[128,2048]{1,0:T(8,128)(2,1)S(1)} %collective-permute-done.low_ref, bf16[288,2048]{1,0:T(8,128)(2,1)S(1)} %copy-done, ...), custom_call_target="tpu_custom_call" | custom-call | flops 6000000000 | bytes 23437500 | tf_op jit(solution)/shard_map/pallas_call | solution.py:287
  53.5 7.1 %shard_map.131 = bf16[288,2048]{1,0:T(8,128)(2,1)} custom-call(s32[1]{0:T(128)} %bitcast.start_ref, f32[8]{0:T(128)S(1)} %copy-done.11, bf16[3,8,96,128]{3,2,1,0:T(8,128)(2,1)S(1)} %get-tuple-element.19.q_ref, bf16[544,256]{1,0:T(8,128)(2,1)S(1)} %get-tuple-element.20.k_ref, bf16[544,256]{1,0:T(8,128)(2,1)S(1)} %get-tuple-element.21.v_ref, ...), custom_call_target="tpu_custom_call" | custom-call | flops 3000000000 | bytes 11718750 | tf_op jit(solution)/shard_map/pallas_call | solution.py:287
  (36 shorter events, 0.6 us)
Async XLA Ops:
  1.8 18.6 %all-to-all-start = ((bf16[16,8,768]{2,1,0:T(8,128)(2,1)}), bf16[16,8,768]{2,1,0:T(8,128)(2,1)}, u32[]{:S(2)}, u32[]{:S(2)}) async-start(bf16[16,8,768]{2,1,0:T(8,128)(2,1)} %shard_map.127), calls=%async_computation | async-start | bytes 393216 | tf_op jit(solution)/shard_map/first/all_to_all | solution.py:44
  12.6 35.8 %collective-permute-start = (bf16[128,2048]{1,0:T(8,128)(2,1)}, bf16[128,2048]{1,0:T(8,128)(2,1)S(1)}, u32[]{:S(2)}, u32[]{:S(2)}) collective-permute-start(bf16[128,2048]{1,0:T(8,128)(2,1)} %get-tuple-element.14), channel_id=1, source_target_pairs={{0,1},{1,2},{2,3},{3,4},{4,5},{5,6},{6,7},{7,8},{8,9},{9,10},{10,1... | collective-permute-start | bytes 1572872 | tf_op jit(solution)/shard_map/halo/ppermute | solution.py:381
  14.9 33.5 %collective-permute-start.1 = (bf16[128,2048]{1,0:T(8,128)(2,1)}, bf16[128,2048]{1,0:T(8,128)(2,1)S(1)}, u32[]{:S(2)}, u32[]{:S(2)}) collective-permute-start(bf16[128,2048]{1,0:T(8,128)(2,1)} %get-tuple-element.15), channel_id=1, source_target_pairs={{1,0},{2,1},{3,2},{4,3},{5,4},{6,5},{7,6},{8,7},{9,8},{10,9},{11,1... | collective-permute-start | bytes 1572872 | tf_op jit(solution)/shard_map/halo/ppermute | solution.py:382
  22.1 17.0 %all-to-all-start.1 = ((bf16[16,8,768]{2,1,0:T(8,128)(2,1)}), bf16[16,8,768]{2,1,0:T(8,128)(2,1)S(1)}, u32[]{:S(2)}, u32[]{:S(2)}) async-start(bf16[16,8,768]{2,1,0:T(8,128)(2,1)} %get-tuple-element.16), calls=%async_computation.1 | async-start | bytes 393216 | tf_op jit(solution)/shard_map/second/all_to_all | solution.py:44
  29.6 6.6 %collective-permute-start.4 = (bf16[16,2048]{1,0:T(8,128)(2,1)S(1)}, bf16[16,2048]{1,0:T(8,128)(2,1)S(1)}, u32[]{:S(2)}, u32[]{:S(2)}) collective-permute-start(bf16[16,2048]{1,0:T(8,128)(2,1)S(1)} %get-tuple-element.17.c0_ref), channel_id=1, source_target_pairs={{0,24},{8,0},{16,8},{24,16},{1,25},{9,1},{17,9},{25,17},{2,26},{10... | collective-permute-start | bytes 196616 | tf_op jit(solution)/shard_map/rows/ppermute | solution.py:320
  32.3 6.1 %collective-permute-start.3 = (bf16[16,2048]{1,0:T(8,128)(2,1)S(1)}, bf16[16,2048]{1,0:T(8,128)(2,1)S(1)}, u32[]{:S(2)}, u32[]{:S(2)}) collective-permute-start(bf16[16,2048]{1,0:T(8,128)(2,1)S(1)} %get-tuple-element.17.c0_ref), channel_id=1, source_target_pairs={{0,16},{8,24},{16,0},{24,8},{1,17},{9,25},{17,1},{25,9},{2,18},{10... | collective-permute-start | bytes 196616 | tf_op jit(solution)/shard_map/rows/ppermute | solution.py:320
  33.2 5.9 %collective-permute-start.2 = (bf16[16,2048]{1,0:T(8,128)(2,1)S(1)}, bf16[16,2048]{1,0:T(8,128)(2,1)S(1)}, u32[]{:S(2)}, u32[]{:S(2)}) collective-permute-start(bf16[16,2048]{1,0:T(8,128)(2,1)S(1)} %get-tuple-element.17.c0_ref), channel_id=1, source_target_pairs={{0,8},{8,16},{16,24},{24,0},{1,9},{9,17},{17,25},{25,1},{2,10},{10... | collective-permute-start | bytes 196616 | tf_op jit(solution)/shard_map/rows/ppermute | solution.py:320
  39.1 1.2 %copy-start.3 = (bf16[2048,256]{1,0:T(8,128)(2,1)S(1)}, bf16[2048,256]{1,0:T(8,128)(2,1)}, u32[]{:S(2)}) copy-start(bf16[2048,256]{1,0:T(8,128)(2,1)} %wk_ref.3) | copy-start | bytes 3145732
  40.4 1.2 %copy-start.5 = (bf16[2048,256]{1,0:T(8,128)(2,1)S(1)}, bf16[2048,256]{1,0:T(8,128)(2,1)}, u32[]{:S(2)}) copy-start(bf16[2048,256]{1,0:T(8,128)(2,1)} %wv_ref.3) | copy-start | bytes 3145732
  41.6 0.7 %copy-start.7 = (f32[2048]{0:T(1024)S(1)}, f32[2048]{0:T(1024)}, u32[]{:S(2)}) copy-start(f32[2048]{0:T(1024)} %param.18) | copy-start | bytes 24580
  42.3 0.7 %copy-start.8 = (f32[128]{0:T(128)S(1)}, f32[128]{0:T(128)}, u32[]{:S(2)}) copy-start(f32[128]{0:T(128)} %param.24) | copy-start | bytes 1540
  42.9 5.5 %copy-start = (bf16[288,2048]{1,0:T(8,128)(2,1)S(1)}, bf16[288,2048]{1,0:T(8,128)(2,1)}, u32[]{:S(2)}) copy-start(bf16[288,2048]{1,0:T(8,128)(2,1)} %lat_ref.1) | copy-start | bytes 3538948
  42.9 5.5 %copy-start.1 = (bf16[2048,1024]{1,0:T(8,128)(2,1)S(1)}, bf16[2048,1024]{1,0:T(8,128)(2,1)}, u32[]{:S(2)}) copy-start(bf16[2048,1024]{1,0:T(8,128)(2,1)} %wq_hbm.1) | copy-start | bytes 12582916
  42.9 5.5 %copy-start.4 = (bf16[2048,256]{1,0:T(8,128)(2,1)S(1)}, bf16[2048,256]{1,0:T(8,128)(2,1)}, u32[]{:S(2)}) copy-start(bf16[2048,256]{1,0:T(8,128)(2,1)} %wk_ref.3) | copy-start | bytes 3145732
  42.9 5.5 %copy-start.6 = (bf16[2048,256]{1,0:T(8,128)(2,1)S(1)}, bf16[2048,256]{1,0:T(8,128)(2,1)}, u32[]{:S(2)}) copy-start(bf16[2048,256]{1,0:T(8,128)(2,1)} %wv_ref.3) | copy-start | bytes 3145732
  42.9 5.5 %copy-start.9 = (f32[128]{0:T(128)S(1)}, f32[128]{0:T(128)}, u32[]{:S(2)}) copy-start(f32[128]{0:T(128)} %param.24) | copy-start | bytes 1540
  42.9 5.5 %copy-start.10 = (f32[128]{0:T(128)S(1)}, f32[128]{0:T(128)}, u32[]{:S(2)}) copy-start(f32[128]{0:T(128)} %param.23) | copy-start | bytes 1540
  43.7 9.8 %collective-permute-start.7 = (bf16[64,512]{1,0:T(8,128)(2,1)S(1)}, bf16[64,512]{1,0:T(8,128)(2,1)S(1)}, u32[]{:S(2)}, u32[]{:S(2)}) collective-permute-start(bf16[64,512]{1,0:T(8,128)(2,1)S(1)} %get-tuple-element.22.x0_ref), channel_id=1, source_target_pairs={{0,6},{2,0},{4,2},{6,4},{1,7},{3,1},{5,3},{7,5},{8,14},{10,8},{12,... | collective-permute-start | bytes 196616 | tf_op jit(solution)/shard_map/pairs/ppermute | solution.py:320
  44.3 9.2 %collective-permute-start.6 = (bf16[64,512]{1,0:T(8,128)(2,1)S(1)}, bf16[64,512]{1,0:T(8,128)(2,1)S(1)}, u32[]{:S(2)}, u32[]{:S(2)}) collective-permute-start(bf16[64,512]{1,0:T(8,128)(2,1)S(1)} %get-tuple-element.22.x0_ref), channel_id=1, source_target_pairs={{0,4},{2,6},{4,0},{6,2},{1,5},{3,7},{5,1},{7,3},{8,12},{10,14},{12... | collective-permute-start | bytes 196616 | tf_op jit(solution)/shard_map/pairs/ppermute | solution.py:320
  46.7 6.8 %collective-permute-start.5 = (bf16[64,512]{1,0:T(8,128)(2,1)S(1)}, bf16[64,512]{1,0:T(8,128)(2,1)S(1)}, u32[]{:S(2)}, u32[]{:S(2)}) collective-permute-start(bf16[64,512]{1,0:T(8,128)(2,1)S(1)} %get-tuple-element.22.x0_ref), channel_id=1, source_target_pairs={{0,2},{2,4},{4,6},{6,0},{1,3},{3,5},{5,7},{7,1},{8,10},{10,12},{12... | collective-permute-start | bytes 196616 | tf_op jit(solution)/shard_map/pairs/ppermute | solution.py:320
  48.5 5.0 %copy-start.2 = (bf16[1024,2048]{1,0:T(8,128)(2,1)S(1)}, bf16[1024,2048]{1,0:T(8,128)(2,1)}, u32[]{:S(2)}) copy-start(bf16[1024,2048]{1,0:T(8,128)(2,1)} %wo_hbm.1) | copy-start | bytes 12582916
  48.5 5.0 %copy-start.11 = (f32[8]{0:T(128)S(1)}, f32[8]{0:T(128)}, u32[]{:S(2)}) copy-start(f32[8]{0:T(128)} %sink_ref.1) | copy-start | bytes 100

commit v2 on v1

--- a/solution.py
+++ b/solution.py
@@ -1,5 +1,3 @@
-import functools
-
 import jax
 import jax.numpy as jnp
 from jax import lax
@@ -117,12 +115,10 @@
     ctx_out[...] = ctx_ref[...].astype(BF16)
 
 
-def context_kernel(
-    second_ref, c0_ref, c1_ref, c2_ref, c3_ref, gain_ref, wk_ref, wv_ref, kgain_ref,
-    kv_out, vec_out, mod_ref, tmp_ref, hid_ref,
+def vectors_kernel(
+    second_ref, mod_out, tmp_ref
 ):
     members, _, width = second_ref.shape
-    model = gain_ref.shape[1]
     side = 4
     for y in range(side):
         total = second_ref[y].astype(F32)
@@ -131,19 +127,29 @@
         tmp_ref[...] = total
         for c in range(2):
             at = (2 * y + c) * width
-            mod_ref[0:2, at : at + width] = (
+            mod_out[0:2, at : at + width] = (
                 tmp_ref[4 * c : 4 * c + 2, :] + tmp_ref[4 * c + 2 : 4 * c + 4, :]
             )
+
+
+def join_kernel(c0_ref, c1_ref, c2_ref, c3_ref, out_ref):
+    for i, ref in enumerate((c0_ref, c1_ref, c2_ref, c3_ref)):
+        n = ref.shape[0]
+        out_ref[i * n : (i + 1) * n, :] = ref[...]
+
+
+def context_kernel(
+    mod_ref, ctx_ref, gain_ref, wk_ref, wv_ref, kgain_ref, kv_out, vec_out, hid_ref
+):
+    model = gain_ref.shape[1]
     gain = gain_ref[...]
     vec_out[0:1, :] = gain * (1.0 + mod_ref[0:1, model : 2 * model])
     vec_out[1:2, :] = mod_ref[0:1, 0:model]
     vec_out[2:3, :] = mod_ref[0:1, 2 * model : 3 * model]
     scale = gain * (1.0 + mod_ref[1:2, model : 2 * model])
     shift = mod_ref[1:2, 0:model]
-    for i, ref in enumerate((c0_ref, c1_ref, c2_ref, c3_ref)):
-        rows = ref[...].astype(F32)
-        n = rows.shape[0]
-        hid_ref[i * n : (i + 1) * n, :] = (rows * rms_scale(rows) * scale + shift).astype(BF16)
+    rows = ctx_ref[...].astype(F32)
+    hid_ref[...] = (rows * rms_scale(rows) * scale + shift).astype(BF16)
     keys = jnp.dot(hid_ref[...], wk_ref[...], preferred_element_type=F32)
     kv_out[:, KV_HEADS * HEAD :] = jnp.dot(
         hid_ref[...], wv_ref[...], preferred_element_type=F32
@@ -164,12 +170,10 @@
 
 
 def project_kernel(
-    start_ref, low_ref, mid_ref, high_ref, vec_ref, wk_ref, wv_ref, qgain_ref, kgain_ref,
-    row_ref, col_ref, wq_hbm,
-    q_out, k_out, v_out, hid_ref, table_ref, wq_ref, sem,
-):
-    load = pltpu.make_async_copy(wq_hbm, wq_ref, sem)
-    load.start()
+    low_ref, mid_ref, high_ref, vec_ref, wk_ref, wv_ref, qgain_ref, kgain_ref,
+    row_ref, col_ref, wq_ref,
+    q_out, k_out, v_out, hid_ref, table_ref,
+):
     own = mid_ref.shape[0]
     rows = own + 2 * WINDOW
     scale = vec_ref[0:1, :]
@@ -180,7 +184,7 @@
             v = ref[r : r + 32, :].astype(F32)
             hid_ref[at : at + 32, :] = (v * rms_scale(v) * scale + shift).astype(BF16)
             at += 32
-    block = start_ref[0] // GROUP_ROWS - WINDOW // GROUP_ROWS
+    block = lax.axis_index(AXES) * (own // GROUP_ROWS) - WINDOW // GROUP_ROWS
     first_row = lax.shift_right_arithmetic(block, 1)
     for i in range(rows // GROUP_ROWS):
         row = lax.shift_right_arithmetic(block + i, 1) - first_row
@@ -199,7 +203,6 @@
         k = k * rms_scale(k) * kgain
         k_out[:, h * HEAD : (h + 1) * HEAD] = turn(k, table_ref, first, 0, rows // GROUP_ROWS)
     qgain = qgain_ref[...]
-    load.wait()
     for pair in range(HEADS // 2):
         at = pair * 2 * HEAD
         both = jnp.dot(
@@ -215,11 +218,11 @@
 
 
 def attend_kernel(
-    start_ref, sink_ref, q_ref, k_ref, v_ref, x0_ref, x1_ref, x2_ref, x3_ref, lat_ref, vec_ref,
-    wo_hbm, out_ref, mix_ref, vals_ref, ctx_ref, wo_ref, sem, *, total_rows,
-):
-    load = pltpu.make_async_copy(wo_hbm, wo_ref, sem)
-    load.start()
+    sink_ref, q_ref, k_ref, v_ref, x0_ref, x1_ref, x2_ref, x3_ref, lat_ref, vec_ref,
+    wo_ref, out_hbm, mix_ref, vals_ref, ctx_ref, out_ref, out_sems,
+):
+    start = lax.axis_index(AXES) * lat_ref.shape[0]
+    total_rows = lat_ref.shape[0] * lax.axis_size(AXES)
     chunks = q_ref.shape[0]
     rows = k_ref.shape[0]
     far = ctx_ref.shape[0]
@@ -237,7 +240,7 @@
     col = lax.broadcasted_iota(jnp.int32, (CHUNK, width), 1)
     nt = (((1,), (1,)), ((), ()))
     for c in range(chunks):
-        pos = start_ref[0] - WINDOW + c * CHUNK + col
+        pos = start - WINDOW + c * CHUNK + col
         allowed = (col >= row) & (col <= row + 2 * WINDOW) & (pos >= 0) & (pos < total_rows)
         bias = jnp.where(allowed, 0.0, FAR_LOGIT)
         for g in range(KV_HEADS):
@@ -249,7 +252,11 @@
                 q, ctx_ref[:, g * HEAD : (g + 1) * HEAD], nt, preferred_element_type=F32
             ).reshape(GROUP, CHUNK, far)
             sink = jnp.concatenate(
-                [jnp.full((1, CHUNK, 1), sink_ref[g * GROUP + h], F32) for h in range(GROUP)], axis=0
+                [
+                    jnp.broadcast_to(sink_ref[:, g * GROUP + h : g * GROUP + h + 1], (CHUNK, 1))[None]
+                    for h in range(GROUP)
+                ],
+                axis=0,
             ) * (HEAD**0.5)
             top = jnp.maximum(
                 jnp.maximum(
@@ -270,32 +277,42 @@
                     h * CHUNK : (h + 1) * CHUNK
                 ]
     model = out_ref.shape[1]
-    load.wait()
-    for at in range(0, model, 256):
-        update = jnp.dot(mix_ref[...], wo_ref[:, at : at + 256], preferred_element_type=F32)
-        out_ref[:, at : at + 256] = (
-            lat_ref[:, at : at + 256].astype(F32) + vec_ref[2:3, at : at + 256] * update
+    step = 256
+    copies = []
+    for i, at in enumerate(range(0, model, step)):
+        update = jnp.dot(mix_ref[...], wo_ref[:, at : at + step], preferred_element_type=F32)
+        out_ref[:, at : at + step] = (
+            lat_ref[:, at : at + step].astype(F32) + vec_ref[2:3, at : at + step] * update
         ).astype(BF16)
-
-
-def call(kernel, outs, scratch, limit, flops, *args, smem=0, hbm=()):
+        columns = pl.ds(at, step)
+        copy = pltpu.make_async_copy(
+            out_ref.at[:, columns], out_hbm.at[:, columns], out_sems.at[i]
+        )
+        copy.start()
+        copies.append(copy)
+    for copy in copies:
+        copy.wait()
+
+
+def call(kernel, outs, scratch, limit, flops, *args, hbm=(), out_hbm=False):
     vmem = pl.BlockSpec(memory_space=pltpu.VMEM)
     many = isinstance(outs, (list, tuple))
-    specs = [pl.BlockSpec(memory_space=pltpu.SMEM)] * smem + [vmem] * (len(args) - smem)
+    specs = [vmem] * len(args)
+    out_spec = pl.BlockSpec(memory_space=pltpu.HBM) if out_hbm else vmem
     for i in hbm:
         specs[i] = pl.BlockSpec(memory_space=pltpu.HBM)
     return pl.pallas_call(
         kernel,
         out_shape=outs,
         in_specs=specs,
-        out_specs=[vmem] * len(outs) if many else vmem,
+        out_specs=[vmem] * len(outs) if many else out_spec,
         scratch_shapes=scratch,
         compiler_params=pltpu.CompilerParams(vmem_limit_bytes=limit),
         cost_estimate=pl.CostEstimate(flops=flops, bytes_accessed=flops // 256, transcendentals=0),
     )(*args)
 
 
-def rotary_tables(first_row, rows):
+def rotary_tables(row_positions, col_positions):
     quarter = HEAD // 4
     inverse = jnp.power(ROPE_BASE, -jnp.arange(quarter, dtype=F32) / quarter)
     sign = jnp.where(jnp.arange(HEAD // 2) < HEAD // 4, -1.0, 1.0)
@@ -305,8 +322,8 @@
         angles = jnp.concatenate([angles, angles], axis=-1)
         return jnp.stack([jnp.cos(angles), jnp.sin(angles) * sign])
 
-    by_rows = table(first_row + jnp.arange(rows, dtype=jnp.int32))
-    by_cols = table(jnp.arange(GRID_W, dtype=jnp.int32))
+    by_rows = table(row_positions)
+    by_cols = table(col_positions)
     none = ((0, 0), (0, 0))
     return (
         jnp.pad(by_rows, (*none, (0, HEAD // 2))),
@@ -343,12 +360,10 @@
     world = lax.axis_size(AXES)
     members = lax.axis_size(FIRST)
     start = lax.axis_index(AXES) * own
-    total_rows = own * world
     up = [(i, i + 1) for i in range(world - 1)]
     down = [(i + 1, i) for i in range(world - 1)]
     struct = jax.ShapeDtypeStruct
     span = own + 2 * WINDOW
-    start_ref = start.astype(jnp.int32)[None]
 
     payload = call(
         partial_kernel,
@@ -366,22 +381,17 @@
         condition[None], context_condition[None], modulation_weight, context,
         hbm=(0, 1, 2, 3),
     )
-    with jax.named_scope("first"):
-        first = exchange(payload, FIRST)
-    with jax.named_scope("edges"):
-        low, high = call(
-            edges_kernel,
-            [struct((WINDOW, model), BF16), struct((WINDOW, model), BF16)],
-            [pltpu.SemaphoreType.DMA((2,))],
-            ALL_VMEM, 1000,
-            latent,
-            hbm=(0,),
-        )
-    with jax.named_scope("halo"):
-        below = lax.ppermute(high, AXES, up)
-        above = lax.ppermute(low, AXES, down)
-    by_rows, by_cols = rotary_tables(lax.div(start - WINDOW, GRID_W), 16)
-
+    first = exchange(payload, FIRST)
+    low, high = call(
+        edges_kernel,
+        [struct((WINDOW, model), BF16), struct((WINDOW, model), BF16)],
+        [pltpu.SemaphoreType.DMA((2,))],
+        ALL_VMEM - 1300 * 1024, 1000,
+        latent,
+        hbm=(0,),
+    )
+    below = lax.ppermute(high, AXES, up)
+    above = lax.ppermute(low, AXES, down)
     payload, ctx_rows = call(
         middle_kernel,
         [struct((lax.axis_size(SECOND), 8, width), BF16), struct((members, model), BF16)],
@@ -389,23 +399,33 @@
         4 * MIB, 1000,
         first,
     )
-    with jax.named_scope("second"):
-        second = exchange(payload, SECOND)
-    with jax.named_scope("rows"):
-        ctx_parts = spread(ctx_rows, "x")
+    second = exchange(payload, SECOND)
+    ctx_parts = spread(ctx_rows, "x")
+    ctx_rows = call(join_kernel, struct((4 * members, model), BF16), [], 2 * MIB, 1000, *ctx_parts)
+    modulation = call(
+        vectors_kernel,
+        struct((8, 3 * model), F32),
+        [pltpu.VMEM((8, width), F32)],
+        4 * MIB, 4_000_000_000,
+        second,
+    )
+    first_row = lax.div(start - WINDOW, GRID_W).astype(jnp.int32)
+    modulation, row_positions, col_positions = lax.optimization_barrier(
+        (
+            modulation,
+            first_row + jnp.arange(16, dtype=jnp.int32),
+            jnp.arange(GRID_W, dtype=jnp.int32),
+        )
+    )
+    by_rows, by_cols = rotary_tables(row_positions, col_positions)
     ctx_kv, vectors = call(
         context_kernel,
         [struct((4 * members, 2 * kv), BF16), struct((8, model), F32)],
-        [
-            pltpu.VMEM((8, 3 * model), F32),
-            pltpu.VMEM((8, width), F32),
-            pltpu.VMEM((4 * members, model), BF16),
-        ],
+        [pltpu.VMEM((4 * members, model), BF16)],
         8 * MIB, 4_000_000_000,
-        second, *ctx_parts, norm_gain[None], key_weight, value_weight, key_gain[None],
-    )
-    with jax.named_scope("pairs"):
-        ctx_all = spread(ctx_kv, "y")
+        modulation, ctx_rows, norm_gain[None], key_weight, value_weight, key_gain[None],
+    )
+    ctx_all = spread(ctx_kv, "y")
     queries, keys, values = call(
         project_kernel,
         [
@@ -416,27 +436,24 @@
         [
             pltpu.VMEM((span, model), BF16),
             pltpu.VMEM((2, span, HEAD), F32),
-            pltpu.VMEM(query_weight.shape, BF16),
-            pltpu.SemaphoreType.DMA,
         ],
         20 * MIB, 6_000_000_000,
-        start_ref, below, latent, above, vectors, key_weight, value_weight,
-        query_gain[None], key_gain[None], by_rows, by_cols, query_weight,
-        smem=1, hbm=(11,),
+        below, latent, above, vectors, key_weight, value_weight, query_gain[None], key_gain[None],
+        by_rows, by_cols, query_weight,
     )
     return call(
-        functools.partial(attend_kernel, total_rows=total_rows),
+        attend_kernel,
         struct((own, model), BF16),
         [
             pltpu.VMEM((own, HEADS * HEAD), BF16),
             pltpu.VMEM((KV_HEADS, span + world, 2 * HEAD), BF16),
             pltpu.VMEM((world, 2 * kv), BF16),
-            pltpu.VMEM(output_weight.shape, BF16),
-            pltpu.SemaphoreType.DMA,
+            pltpu.VMEM((own, model), BF16),
+            pltpu.SemaphoreType.DMA((8,)),
         ],
         20 * MIB, 3_000_000_000,
-        start_ref, sink_logit, queries, keys, values, *ctx_all, latent, vectors, output_weight,
-        smem=2, hbm=(11,),
+        sink_logit[None], queries, keys, values, *ctx_all, latent, vectors, output_weight,
+        out_hbm=True,
     )
 
 

time: 61.3 us -> 57.3 us (0.935)
  local copies, waits for them, and re-layouts: 3.84 us -> 1.46 us
  Pallas kernels: 18.4 us -> 16.5 us
    unnamed x24 -> x18, local copies, waits for them, and re-layouts: 3.84 us -> 1.46 us
    pallas_call x6 -> x8, Pallas kernels: 18.4 us -> 16.5 us  [call(): pl.pallas_call(kernel, out_shape=outs, in_specs=specs, out_specs=[vmem] *...]
  transfers between devices with their start and end apart: 10 -> 10, of which waited for: 4 -> 4; matrix products, arithmetic and copies ran while one was open for 1% -> 1% of each run, Pallas kernels for 16% -> 15%
where the time goes in v2:
time: 57.3 us; the launch traced here: 56.9 us
  starting transfers between devices  30.8 us (54%)
  Pallas kernels  16.5 us (29%)
  waiting for transfers between devices  7.16 us (12%)
  local copies, waits for them, and re-layouts  1.46 us (3%)
  other arithmetic  0.59 us (1%)
    pallas_call x8, Pallas kernels, call(): pl.pallas_call(kernel, out_shape=outs, in_specs=specs, out_specs=[vmem] *...  16.5 us
    all_to_all x2, starting transfers between devices, exchange(): return lax.all_to_all(array, axes, split_axis=0, concat_axis=0, tiled=True)  16 us
    ppermute x6, starting transfers between devices, spread(): lax.ppermute(array, axis, [(i, (i + k) % size) for i in range(size)])  9.25 us
    ppermute x6, waiting for transfers between devices, spread(): lax.ppermute(array, axis, [(i, (i + k) % size) for i in range(size)])  5.09 us
    ppermute x1, starting transfers between devices, local(): above = lax.ppermute(low, AXES, down)  3.25 us
    ppermute x1, starting transfers between devices, local(): below = lax.ppermute(high, AXES, up)  2.31 us
    all_to_all x2, waiting for transfers between devices, exchange(): return lax.all_to_all(array, axes, split_axis=0, concat_axis=0, tiled=True)  2.07 us
    unnamed x18, local copies, waits for them, and re-layouts  1.46 us
  transfers between devices with their start and end apart: 10, of which 4 were waited for; matrix products, arithmetic and copies ran while one was open for 1% of the time, Pallas kernels for 15%

profile of v2, /device:TPU:8, one launch (start us, length us, event | category | flops | bytes accessed | tf_op | source)
XLA Modules:
  0.0 56.9 jit_solution(230811745908210586)
XLA Ops:
  0.0 1.8 %shard_map.128 = bf16[16,8,768]{2,1,0:T(8,128)(2,1)} custom-call(f32[1,64]{1,0:T(1,128)} %bitcast.15, f32[1,64]{1,0:T(1,128)} %bitcast.16, bf16[64,768]{1,0:T(8,128)(2,1)} %weight_hbm.1, bf16[1,2048]{1,0:T(2,128)(2,1)} %ctx_hbm.1), custom_call_target="tpu_custom_call" | custom-call | flops 1000 | bytes 3 | tf_op jit(solution)/shard_map/pallas_call | solution.py:304
  1.8 8.6 %all-to-all-start = ((bf16[16,8,768]{2,1,0:T(8,128)(2,1)}), bf16[16,8,768]{2,1,0:T(8,128)(2,1)S(1)}, u32[]{:S(2)}, u32[]{:S(2)}) async-start(bf16[16,8,768]{2,1,0:T(8,128)(2,1)} %shard_map.128), calls=%async_computation | async-start | bytes 393216 | tf_op jit(solution)/shard_map/all_to_all | solution.py:42
  10.4 2.2 %shard_map.127 = (bf16[128,2048]{1,0:T(8,128)(2,1)}, bf16[128,2048]{1,0:T(8,128)(2,1)}) custom-call(bf16[288,2048]{1,0:T(8,128)(2,1)} %lat_ref.1), custom_call_target="tpu_custom_call" | custom-call | flops 1000 | bytes 3 | tf_op jit(solution)/shard_map/pallas_call | solution.py:304
  12.6 2.3 %collective-permute-start = (bf16[128,2048]{1,0:T(8,128)(2,1)}, bf16[128,2048]{1,0:T(8,128)(2,1)S(1)}, u32[]{:S(2)}, u32[]{:S(2)}) collective-permute-start(bf16[128,2048]{1,0:T(8,128)(2,1)} %get-tuple-element.17), channel_id=1, source_target_pairs={{0,1},{1,2},{2,3},{3,4},{4,5},{5,6},{6,7},{7,8},{8,9},{9,10},{10,1... | collective-permute-start | bytes 1572872 | tf_op jit(solution)/shard_map/ppermute | solution.py:393
  14.9 3.3 %collective-permute-start.1 = (bf16[128,2048]{1,0:T(8,128)(2,1)}, bf16[128,2048]{1,0:T(8,128)(2,1)}, u32[]{:S(2)}, u32[]{:S(2)}) collective-permute-start(bf16[128,2048]{1,0:T(8,128)(2,1)} %get-tuple-element.18), channel_id=1, source_target_pairs={{1,0},{2,1},{3,2},{4,3},{5,4},{6,5},{7,6},{8,7},{9,8},{10,9},{11,1... | collective-permute-start | bytes 1572872 | tf_op jit(solution)/shard_map/ppermute | solution.py:394
  18.2 2.1 %all-to-all-done.in_ref = bf16[16,8,768]{2,1,0:T(8,128)(2,1)S(1)} async-done(((bf16[16,8,768]{2,1,0:T(8,128)(2,1)}), bf16[16,8,768]{2,1,0:T(8,128)(2,1)S(1)}, u32[]{:S(2)}, u32[]{:S(2)}) %all-to-all-start) | async-done | bytes 196640 | tf_op jit(solution)/shard_map/all_to_all | solution.py:42
  20.3 0.8 %shard_map.129 = (bf16[16,8,768]{2,1,0:T(8,128)(2,1)}, bf16[16,2048]{1,0:T(8,128)(2,1)S(1)}) custom-call(bf16[16,8,768]{2,1,0:T(8,128)(2,1)S(1)} %all-to-all-done.in_ref), custom_call_target="tpu_custom_call" | custom-call | flops 1000 | bytes 3 | tf_op jit(solution)/shard_map/pallas_call | solution.py:304
  21.0 7.4 %all-to-all-start.1 = ((bf16[16,8,768]{2,1,0:T(8,128)(2,1)}), bf16[16,8,768]{2,1,0:T(8,128)(2,1)S(1)}, u32[]{:S(2)}, u32[]{:S(2)}) async-start(bf16[16,8,768]{2,1,0:T(8,128)(2,1)} %get-tuple-element.19), calls=%async_computation.1 | async-start | bytes 393216 | tf_op jit(solution)/shard_map/all_to_all | solution.py:42
  28.4 2.8 %collective-permute-start.4 = (bf16[16,2048]{1,0:T(8,128)(2,1)S(1)}, bf16[16,2048]{1,0:T(8,128)(2,1)S(1)}, u32[]{:S(2)}, u32[]{:S(2)}) collective-permute-start(bf16[16,2048]{1,0:T(8,128)(2,1)S(1)} %get-tuple-element.21.c0_ref), channel_id=1, source_target_pairs={{0,24},{8,0},{16,8},{24,16},{1,25},{9,1},{17,9},{25,17},{2,26},{10... | collective-permute-start | bytes 196616 | tf_op jit(solution)/shard_map/ppermute | solution.py:337
  31.2 0.9 %collective-permute-start.3 = (bf16[16,2048]{1,0:T(8,128)(2,1)S(1)}, bf16[16,2048]{1,0:T(8,128)(2,1)S(1)}, u32[]{:S(2)}, u32[]{:S(2)}) collective-permute-start(bf16[16,2048]{1,0:T(8,128)(2,1)S(1)} %get-tuple-element.21.c0_ref), channel_id=1, source_target_pairs={{0,16},{8,24},{16,0},{24,8},{1,17},{9,25},{17,1},{25,9},{2,18},{10... | collective-permute-start | bytes 196616 | tf_op jit(solution)/shard_map/ppermute | solution.py:337
  32.0 0.9 %collective-permute-start.2 = (bf16[16,2048]{1,0:T(8,128)(2,1)S(1)}, bf16[16,2048]{1,0:T(8,128)(2,1)S(1)}, u32[]{:S(2)}, u32[]{:S(2)}) collective-permute-start(bf16[16,2048]{1,0:T(8,128)(2,1)S(1)} %get-tuple-element.21.c0_ref), channel_id=1, source_target_pairs={{0,8},{8,16},{16,24},{24,0},{1,9},{9,17},{17,25},{25,1},{2,10},{10... | collective-permute-start | bytes 196616 | tf_op jit(solution)/shard_map/ppermute | solution.py:337
  32.9 2.2 %collective-permute-done.4.c3_ref = bf16[16,2048]{1,0:T(8,128)(2,1)S(1)} collective-permute-done((bf16[16,2048]{1,0:T(8,128)(2,1)S(1)}, bf16[16,2048]{1,0:T(8,128)(2,1)S(1)}, u32[]{:S(2)}, u32[]{:S(2)}) %collective-permute-start.4) | collective-permute-done | bytes 65568 | tf_op jit(solution)/shard_map/ppermute | solution.py:337
  35.1 2.1 %collective-permute-done.3.c2_ref = bf16[16,2048]{1,0:T(8,128)(2,1)S(1)} collective-permute-done((bf16[16,2048]{1,0:T(8,128)(2,1)S(1)}, bf16[16,2048]{1,0:T(8,128)(2,1)S(1)}, u32[]{:S(2)}, u32[]{:S(2)}) %collective-permute-start.3) | collective-permute-done | bytes 65568 | tf_op jit(solution)/shard_map/ppermute | solution.py:337
  37.3 0.7 %collective-permute-done.2.c1_ref = bf16[16,2048]{1,0:T(8,128)(2,1)S(1)} collective-permute-done((bf16[16,2048]{1,0:T(8,128)(2,1)S(1)}, bf16[16,2048]{1,0:T(8,128)(2,1)S(1)}, u32[]{:S(2)}, u32[]{:S(2)}) %collective-permute-start.2) | collective-permute-done | bytes 65568 | tf_op jit(solution)/shard_map/ppermute | solution.py:337
  38.1 1.1 %copy-done.3 = bf16[2048,256]{1,0:T(8,128)(2,1)S(1)} copy-done((bf16[2048,256]{1,0:T(8,128)(2,1)S(1)}, bf16[2048,256]{1,0:T(8,128)(2,1)}, u32[]{:S(2)}) %copy-start.3) | copy-done | bytes 1048600
  39.2 0.3 copy-done.4
  39.6 0.7 %shard_map.132 = (bf16[64,512]{1,0:T(8,128)(2,1)S(1)}, f32[8,2048]{1,0:T(8,128)S(1)}) custom-call(f32[8,6144]{1,0:T(8,128)S(1)} %shard_map.130.mod_ref, bf16[64,2048]{1,0:T(8,128)(2,1)S(1)} %shard_map.131.ctx_ref, f32[1,2048]{1,0:T(1,128)S(1)} %bitcast.10, bf16[2048,256]{1,0:T(8,128)(2,1)S(1)} %copy-done.3, bf16[2048,256]{1,0:T(8,128)(2,1)S(1)} %copy-done.4, ...), custom_call_target="tpu_custom_call" | custom-call | flops 4000000000 | bytes 15625000 | tf_op jit(solution)/shard_map/pallas_call | solution.py:304
  40.2 0.6 %collective-permute-start.7 = (bf16[64,512]{1,0:T(8,128)(2,1)S(1)}, bf16[64,512]{1,0:T(8,128)(2,1)S(1)}, u32[]{:S(2)}, u32[]{:S(2)}) collective-permute-start(bf16[64,512]{1,0:T(8,128)(2,1)S(1)} %get-tuple-element.28.x0_ref), channel_id=1, source_target_pairs={{0,6},{2,0},{4,2},{6,4},{1,7},{3,1},{5,3},{7,5},{8,14},{10,8},{12,... | collective-permute-start | bytes 196616 | tf_op jit(solution)/shard_map/ppermute | solution.py:337
  40.9 2.4 %collective-permute-start.6 = (bf16[64,512]{1,0:T(8,128)(2,1)S(1)}, bf16[64,512]{1,0:T(8,128)(2,1)S(1)}, u32[]{:S(2)}, u32[]{:S(2)}) collective-permute-start(bf16[64,512]{1,0:T(8,128)(2,1)S(1)} %get-tuple-element.28.x0_ref), channel_id=1, source_target_pairs={{0,4},{2,6},{4,0},{6,2},{1,5},{3,7},{5,1},{7,3},{8,12},{10,14},{12... | collective-permute-start | bytes 196616 | tf_op jit(solution)/shard_map/ppermute | solution.py:337
  43.2 1.8 %collective-permute-start.5 = (bf16[64,512]{1,0:T(8,128)(2,1)S(1)}, bf16[64,512]{1,0:T(8,128)(2,1)S(1)}, u32[]{:S(2)}, u32[]{:S(2)}) collective-permute-start(bf16[64,512]{1,0:T(8,128)(2,1)S(1)} %get-tuple-element.28.x0_ref), channel_id=1, source_target_pairs={{0,2},{2,4},{4,6},{6,0},{1,3},{3,5},{5,7},{7,1},{8,10},{10,12},{12... | collective-permute-start | bytes 196616 | tf_op jit(solution)/shard_map/ppermute | solution.py:337
  45.1 0.1 fusion.1
  45.3 0.2 fusion
  45.7 5.0 %shard_map.133 = (bf16[3,8,96,128]{3,2,1,0:T(8,128)(2,1)S(1)}, bf16[544,256]{1,0:T(8,128)(2,1)S(1)}, bf16[544,256]{1,0:T(8,128)(2,1)S(1)}) custom-call(bf16[128,2048]{1,0:T(8,128)(2,1)S(1)} %collective-permute-done.low_ref, bf16[288,2048]{1,0:T(8,128)(2,1)S(1)} %copy-done, bf16[128,2048]{1,0:T(8,128)(2,1)} %collective-permute-done.1.high_ref, ...), custom_call_target="tpu_custom_call" | custom-call | flops 6000000000 | bytes 23437500 | tf_op jit(solution)/shard_map/pallas_call | solution.py:304
  50.8 6.0 %shard_map.134 = bf16[288,2048]{1,0:T(8,128)(2,1)} custom-call(f32[1,8]{1,0:T(1,128)S(1)} %bitcast.14, bf16[3,8,96,128]{3,2,1,0:T(8,128)(2,1)S(1)} %get-tuple-element.25.q_ref, bf16[544,256]{1,0:T(8,128)(2,1)S(1)} %get-tuple-element.26.k_ref, bf16[544,256]{1,0:T(8,128)(2,1)S(1)} %get-tuple-element.27.v_ref, bf16[64,512]{1,0:T(8,128)(2,1)S(1)} %get-tuple-element.28.x0_ref, ...), custom_call_target="tpu_custom_call" | custom-call | flops 3000000000 | bytes 11718750 | tf_op jit(solution)/shard_map/pallas_call | solution.py:304
  (34 shorter events, 0.4 us)
Async XLA Ops:
  1.8 18.5 %all-to-all-start = ((bf16[16,8,768]{2,1,0:T(8,128)(2,1)}), bf16[16,8,768]{2,1,0:T(8,128)(2,1)S(1)}, u32[]{:S(2)}, u32[]{:S(2)}) async-start(bf16[16,8,768]{2,1,0:T(8,128)(2,1)} %shard_map.128), calls=%async_computation | async-start | bytes 393216 | tf_op jit(solution)/shard_map/all_to_all | solution.py:42
  12.6 33.0 %collective-permute-start = (bf16[128,2048]{1,0:T(8,128)(2,1)}, bf16[128,2048]{1,0:T(8,128)(2,1)S(1)}, u32[]{:S(2)}, u32[]{:S(2)}) collective-permute-start(bf16[128,2048]{1,0:T(8,128)(2,1)} %get-tuple-element.17), channel_id=1, source_target_pairs={{0,1},{1,2},{2,3},{3,4},{4,5},{5,6},{6,7},{7,8},{8,9},{9,10},{10,1... | collective-permute-start | bytes 1572872 | tf_op jit(solution)/shard_map/ppermute | solution.py:393
  14.9 30.7 %collective-permute-start.1 = (bf16[128,2048]{1,0:T(8,128)(2,1)}, bf16[128,2048]{1,0:T(8,128)(2,1)}, u32[]{:S(2)}, u32[]{:S(2)}) collective-permute-start(bf16[128,2048]{1,0:T(8,128)(2,1)} %get-tuple-element.18), channel_id=1, source_target_pairs={{1,0},{2,1},{3,2},{4,3},{5,4},{6,5},{7,6},{8,7},{9,8},{10,9},{11,1... | collective-permute-start | bytes 1572872 | tf_op jit(solution)/shard_map/ppermute | solution.py:394
  21.0 17.0 %all-to-all-start.1 = ((bf16[16,8,768]{2,1,0:T(8,128)(2,1)}), bf16[16,8,768]{2,1,0:T(8,128)(2,1)S(1)}, u32[]{:S(2)}, u32[]{:S(2)}) async-start(bf16[16,8,768]{2,1,0:T(8,128)(2,1)} %get-tuple-element.19), calls=%async_computation.1 | async-start | bytes 393216 | tf_op jit(solution)/shard_map/all_to_all | solution.py:42
  28.4 6.7 %collective-permute-start.4 = (bf16[16,2048]{1,0:T(8,128)(2,1)S(1)}, bf16[16,2048]{1,0:T(8,128)(2,1)S(1)}, u32[]{:S(2)}, u32[]{:S(2)}) collective-permute-start(bf16[16,2048]{1,0:T(8,128)(2,1)S(1)} %get-tuple-element.21.c0_ref), channel_id=1, source_target_pairs={{0,24},{8,0},{16,8},{24,16},{1,25},{9,1},{17,9},{25,17},{2,26},{10... | collective-permute-start | bytes 196616 | tf_op jit(solution)/shard_map/ppermute | solution.py:337
  31.2 6.1 %collective-permute-start.3 = (bf16[16,2048]{1,0:T(8,128)(2,1)S(1)}, bf16[16,2048]{1,0:T(8,128)(2,1)S(1)}, u32[]{:S(2)}, u32[]{:S(2)}) collective-permute-start(bf16[16,2048]{1,0:T(8,128)(2,1)S(1)} %get-tuple-element.21.c0_ref), channel_id=1, source_target_pairs={{0,16},{8,24},{16,0},{24,8},{1,17},{9,25},{17,1},{25,9},{2,18},{10... | collective-permute-start | bytes 196616 | tf_op jit(solution)/shard_map/ppermute | solution.py:337
  32.0 5.9 %collective-permute-start.2 = (bf16[16,2048]{1,0:T(8,128)(2,1)S(1)}, bf16[16,2048]{1,0:T(8,128)(2,1)S(1)}, u32[]{:S(2)}, u32[]{:S(2)}) collective-permute-start(bf16[16,2048]{1,0:T(8,128)(2,1)S(1)} %get-tuple-element.21.c0_ref), channel_id=1, source_target_pairs={{0,8},{8,16},{16,24},{24,0},{1,9},{9,17},{17,25},{25,1},{2,10},{10... | collective-permute-start | bytes 196616 | tf_op jit(solution)/shard_map/ppermute | solution.py:337
  38.0 1.2 %copy-start.3 = (bf16[2048,256]{1,0:T(8,128)(2,1)S(1)}, bf16[2048,256]{1,0:T(8,128)(2,1)}, u32[]{:S(2)}) copy-start(bf16[2048,256]{1,0:T(8,128)(2,1)} %wk_ref.3) | copy-start | bytes 3145732
  38.0 1.5 %copy-start.4 = (bf16[2048,256]{1,0:T(8,128)(2,1)S(1)}, bf16[2048,256]{1,0:T(8,128)(2,1)}, u32[]{:S(2)}) copy-start(bf16[2048,256]{1,0:T(8,128)(2,1)} %wv_ref.3) | copy-start | bytes 3145732
  38.0 1.5 %copy-start.5 = (f32[2048]{0:T(1024)S(1)}, f32[2048]{0:T(1024)}, u32[]{:S(2)}) copy-start(f32[2048]{0:T(1024)} %param.18) | copy-start | bytes 24580
  38.0 1.5 %copy-start.6 = (f32[128]{0:T(128)S(1)}, f32[128]{0:T(128)}, u32[]{:S(2)}) copy-start(f32[128]{0:T(128)} %param.24) | copy-start | bytes 1540
  39.6 6.1 %copy-start = (bf16[288,2048]{1,0:T(8,128)(2,1)S(1)}, bf16[288,2048]{1,0:T(8,128)(2,1)}, u32[]{:S(2)}) copy-start(bf16[288,2048]{1,0:T(8,128)(2,1)} %lat_ref.1) | copy-start | bytes 3538948
  39.6 6.1 %copy-start.1 = (bf16[2048,1024]{1,0:T(8,128)(2,1)S(1)}, bf16[2048,1024]{1,0:T(8,128)(2,1)}, u32[]{:S(2)}) copy-start(bf16[2048,1024]{1,0:T(8,128)(2,1)} %wq_ref.1) | copy-start | bytes 12582916
  39.6 6.1 %copy-start.7 = (f32[128]{0:T(128)S(1)}, f32[128]{0:T(128)}, u32[]{:S(2)}) copy-start(f32[128]{0:T(128)} %param.23) | copy-start | bytes 1540
  40.2 10.5 %collective-permute-start.7 = (bf16[64,512]{1,0:T(8,128)(2,1)S(1)}, bf16[64,512]{1,0:T(8,128)(2,1)S(1)}, u32[]{:S(2)}, u32[]{:S(2)}) collective-permute-start(bf16[64,512]{1,0:T(8,128)(2,1)S(1)} %get-tuple-element.28.x0_ref), channel_id=1, source_target_pairs={{0,6},{2,0},{4,2},{6,4},{1,7},{3,1},{5,3},{7,5},{8,14},{10,8},{12,... | collective-permute-start | bytes 196616 | tf_op jit(solution)/shard_map/ppermute | solution.py:337
  40.9 9.8 %collective-permute-start.6 = (bf16[64,512]{1,0:T(8,128)(2,1)S(1)}, bf16[64,512]{1,0:T(8,128)(2,1)S(1)}, u32[]{:S(2)}, u32[]{:S(2)}) collective-permute-start(bf16[64,512]{1,0:T(8,128)(2,1)S(1)} %get-tuple-element.28.x0_ref), channel_id=1, source_target_pairs={{0,4},{2,6},{4,0},{6,2},{1,5},{3,7},{5,1},{7,3},{8,12},{10,14},{12... | collective-permute-start | bytes 196616 | tf_op jit(solution)/shard_map/ppermute | solution.py:337
  43.2 7.5 %collective-permute-start.5 = (bf16[64,512]{1,0:T(8,128)(2,1)S(1)}, bf16[64,512]{1,0:T(8,128)(2,1)S(1)}, u32[]{:S(2)}, u32[]{:S(2)}) collective-permute-start(bf16[64,512]{1,0:T(8,128)(2,1)S(1)} %get-tuple-element.28.x0_ref), channel_id=1, source_target_pairs={{0,2},{2,4},{4,6},{6,0},{1,3},{3,5},{5,7},{7,1},{8,10},{10,12},{12... | collective-permute-start | bytes 196616 | tf_op jit(solution)/shard_map/ppermute | solution.py:337
  45.7 5.1 %copy-start.2 = (bf16[1024,2048]{1,0:T(8,128)(2,1)S(1)}, bf16[1024,2048]{1,0:T(8,128)(2,1)}, u32[]{:S(2)}) copy-start(bf16[1024,2048]{1,0:T(8,128)(2,1)} %wo_ref.1) | copy-start | bytes 12582916
  45.7 5.1 %copy-start.8 = (f32[8]{0:T(128)S(1)}, f32[8]{0:T(128)}, u32[]{:S(2)}) copy-start(f32[8]{0:T(128)} %param.25) | copy-start | bytes 100

commit v3 on v2

--- a/solution.py
+++ b/solution.py
@@ -116,8 +116,9 @@
 
 
 def vectors_kernel(
-    second_ref, mod_out, tmp_ref
-):
+    second_ref, low_hbm, mod_out, low_ref, tmp_ref, sems
+):
+    copies = copy_all([(low_hbm, low_ref)], sems)
     members, _, width = second_ref.shape
     side = 4
     for y in range(side):
@@ -130,6 +131,7 @@
             mod_out[0:2, at : at + width] = (
                 tmp_ref[4 * c : 4 * c + 2, :] + tmp_ref[4 * c + 2 : 4 * c + 4, :]
             )
+    copies[0].wait()
 
 
 def join_kernel(c0_ref, c1_ref, c2_ref, c3_ref, out_ref):
@@ -402,12 +404,13 @@
     second = exchange(payload, SECOND)
     ctx_parts = spread(ctx_rows, "x")
     ctx_rows = call(join_kernel, struct((4 * members, model), BF16), [], 2 * MIB, 1000, *ctx_parts)
-    modulation = call(
+    modulation, below = call(
         vectors_kernel,
-        struct((8, 3 * model), F32),
-        [pltpu.VMEM((8, width), F32)],
+        [struct((8, 3 * model), F32), struct((WINDOW, model), BF16)],
+        [pltpu.VMEM((8, width), F32), pltpu.SemaphoreType.DMA((1,))],
         4 * MIB, 4_000_000_000,
-        second,
+        second, below,
+        hbm=(1,),
     )
     first_row = lax.div(start - WINDOW, GRID_W).astype(jnp.int32)
     modulation, row_positions, col_positions = lax.optimization_barrier(

time: 57.3 us -> 56.3 us (0.983)
  local copies, waits for them, and re-layouts: 1.46 us -> 0.48 us
    unnamed x18, local copies, waits for them, and re-layouts: 1.46 us -> 0.47 us
where the time goes in v3:
time: 56.3 us; the launch traced here: 55.9 us
  starting transfers between devices  30.8 us (55%)
  Pallas kernels  16.5 us (29%)
  waiting for transfers between devices  7.16 us (13%)
  other arithmetic  0.59 us (1%)
    pallas_call x8, Pallas kernels, call(): pl.pallas_call(kernel, out_shape=outs, in_specs=specs, out_specs=[vmem] *...  16.5 us
    all_to_all x2, starting transfers between devices, exchange(): return lax.all_to_all(array, axes, split_axis=0, concat_axis=0, tiled=True)  16 us
    ppermute x6, starting transfers between devices, spread(): lax.ppermute(array, axis, [(i, (i + k) % size) for i in range(size)])  9.25 us
    ppermute x6, waiting for transfers between devices, spread(): lax.ppermute(array, axis, [(i, (i + k) % size) for i in range(size)])  5.09 us
    ppermute x1, starting transfers between devices, local(): above = lax.ppermute(low, AXES, down)  3.25 us
    ppermute x1, starting transfers between devices, local(): below = lax.ppermute(high, AXES, up)  2.31 us
    all_to_all x2, waiting for transfers between devices, exchange(): return lax.all_to_all(array, axes, split_axis=0, concat_axis=0, tiled=True)  2.06 us
  transfers between devices with their start and end apart: 10, of which 4 were waited for; matrix products, arithmetic and copies ran while one was open for 1% of the time, Pallas kernels for 15%

profile of v3, /device:TPU:8, one launch (start us, length us, event | category | flops | bytes accessed | tf_op | source)
XLA Modules:
  0.0 55.9 jit_solution(15910306916394346133)
XLA Ops:
  0.0 1.8 %shard_map.127 = bf16[16,8,768]{2,1,0:T(8,128)(2,1)} custom-call(f32[1,64]{1,0:T(1,128)} %bitcast.15, f32[1,64]{1,0:T(1,128)} %bitcast.16, bf16[64,768]{1,0:T(8,128)(2,1)} %weight_hbm.1, bf16[1,2048]{1,0:T(2,128)(2,1)} %ctx_hbm.1), custom_call_target="tpu_custom_call" | custom-call | flops 1000 | bytes 3 | tf_op jit(solution)/shard_map/pallas_call | solution.py:306
  1.8 8.6 %all-to-all-start = ((bf16[16,8,768]{2,1,0:T(8,128)(2,1)}), bf16[16,8,768]{2,1,0:T(8,128)(2,1)S(1)}, u32[]{:S(2)}, u32[]{:S(2)}) async-start(bf16[16,8,768]{2,1,0:T(8,128)(2,1)} %shard_map.127), calls=%async_computation | async-start | bytes 393216 | tf_op jit(solution)/shard_map/all_to_all | solution.py:42
  10.4 2.2 %shard_map.129 = (bf16[128,2048]{1,0:T(8,128)(2,1)}, bf16[128,2048]{1,0:T(8,128)(2,1)}) custom-call(bf16[288,2048]{1,0:T(8,128)(2,1)} %lat_ref.1), custom_call_target="tpu_custom_call" | custom-call | flops 1000 | bytes 3 | tf_op jit(solution)/shard_map/pallas_call | solution.py:306
  12.6 2.3 %collective-permute-start = (bf16[128,2048]{1,0:T(8,128)(2,1)}, bf16[128,2048]{1,0:T(8,128)(2,1)}, u32[]{:S(2)}, u32[]{:S(2)}) collective-permute-start(bf16[128,2048]{1,0:T(8,128)(2,1)} %get-tuple-element.20), channel_id=1, source_target_pairs={{0,1},{1,2},{2,3},{3,4},{4,5},{5,6},{6,7},{7,8},{8,9},{9,10},{10,1... | collective-permute-start | bytes 1572872 | tf_op jit(solution)/shard_map/ppermute | solution.py:395
  14.9 3.2 %collective-permute-start.1 = (bf16[128,2048]{1,0:T(8,128)(2,1)}, bf16[128,2048]{1,0:T(8,128)(2,1)S(1)}, u32[]{:S(2)}, u32[]{:S(2)}) collective-permute-start(bf16[128,2048]{1,0:T(8,128)(2,1)} %get-tuple-element.22), channel_id=1, source_target_pairs={{1,0},{2,1},{3,2},{4,3},{5,4},{6,5},{7,6},{8,7},{9,8},{10,9},{11,1... | collective-permute-start | bytes 1572872 | tf_op jit(solution)/shard_map/ppermute | solution.py:396
  18.2 2.1 %all-to-all-done.in_ref = bf16[16,8,768]{2,1,0:T(8,128)(2,1)S(1)} async-done(((bf16[16,8,768]{2,1,0:T(8,128)(2,1)}), bf16[16,8,768]{2,1,0:T(8,128)(2,1)S(1)}, u32[]{:S(2)}, u32[]{:S(2)}) %all-to-all-start) | async-done | bytes 196640 | tf_op jit(solution)/shard_map/all_to_all | solution.py:42
  20.3 0.8 %shard_map.128 = (bf16[16,8,768]{2,1,0:T(8,128)(2,1)}, bf16[16,2048]{1,0:T(8,128)(2,1)S(1)}) custom-call(bf16[16,8,768]{2,1,0:T(8,128)(2,1)S(1)} %all-to-all-done.in_ref), custom_call_target="tpu_custom_call" | custom-call | flops 1000 | bytes 3 | tf_op jit(solution)/shard_map/pallas_call | solution.py:306
  21.0 7.4 %all-to-all-start.1 = ((bf16[16,8,768]{2,1,0:T(8,128)(2,1)}), bf16[16,8,768]{2,1,0:T(8,128)(2,1)S(1)}, u32[]{:S(2)}, u32[]{:S(2)}) async-start(bf16[16,8,768]{2,1,0:T(8,128)(2,1)} %get-tuple-element.19), calls=%async_computation.1 | async-start | bytes 393216 | tf_op jit(solution)/shard_map/all_to_all | solution.py:42
  28.4 2.8 %collective-permute-start.4 = (bf16[16,2048]{1,0:T(8,128)(2,1)S(1)}, bf16[16,2048]{1,0:T(8,128)(2,1)S(1)}, u32[]{:S(2)}, u32[]{:S(2)}) collective-permute-start(bf16[16,2048]{1,0:T(8,128)(2,1)S(1)} %get-tuple-element.25.c0_ref), channel_id=1, source_target_pairs={{0,24},{8,0},{16,8},{24,16},{1,25},{9,1},{17,9},{25,17},{2,26},{10... | collective-permute-start | bytes 196616 | tf_op jit(solution)/shard_map/ppermute | solution.py:339
  31.2 0.9 %collective-permute-start.3 = (bf16[16,2048]{1,0:T(8,128)(2,1)S(1)}, bf16[16,2048]{1,0:T(8,128)(2,1)S(1)}, u32[]{:S(2)}, u32[]{:S(2)}) collective-permute-start(bf16[16,2048]{1,0:T(8,128)(2,1)S(1)} %get-tuple-element.25.c0_ref), channel_id=1, source_target_pairs={{0,16},{8,24},{16,0},{24,8},{1,17},{9,25},{17,1},{25,9},{2,18},{10... | collective-permute-start | bytes 196616 | tf_op jit(solution)/shard_map/ppermute | solution.py:339
  32.0 0.9 %collective-permute-start.2 = (bf16[16,2048]{1,0:T(8,128)(2,1)S(1)}, bf16[16,2048]{1,0:T(8,128)(2,1)S(1)}, u32[]{:S(2)}, u32[]{:S(2)}) collective-permute-start(bf16[16,2048]{1,0:T(8,128)(2,1)S(1)} %get-tuple-element.25.c0_ref), channel_id=1, source_target_pairs={{0,8},{8,16},{16,24},{24,0},{1,9},{9,17},{17,25},{25,1},{2,10},{10... | collective-permute-start | bytes 196616 | tf_op jit(solution)/shard_map/ppermute | solution.py:339
  32.9 2.2 %collective-permute-done.4.c3_ref = bf16[16,2048]{1,0:T(8,128)(2,1)S(1)} collective-permute-done((bf16[16,2048]{1,0:T(8,128)(2,1)S(1)}, bf16[16,2048]{1,0:T(8,128)(2,1)S(1)}, u32[]{:S(2)}, u32[]{:S(2)}) %collective-permute-start.4) | collective-permute-done | bytes 65568 | tf_op jit(solution)/shard_map/ppermute | solution.py:339
  35.1 2.1 %collective-permute-done.3.c2_ref = bf16[16,2048]{1,0:T(8,128)(2,1)S(1)} collective-permute-done((bf16[16,2048]{1,0:T(8,128)(2,1)S(1)}, bf16[16,2048]{1,0:T(8,128)(2,1)S(1)}, u32[]{:S(2)}, u32[]{:S(2)}) %collective-permute-start.3) | collective-permute-done | bytes 65568 | tf_op jit(solution)/shard_map/ppermute | solution.py:339
  37.3 0.7 %collective-permute-done.2.c1_ref = bf16[16,2048]{1,0:T(8,128)(2,1)S(1)} collective-permute-done((bf16[16,2048]{1,0:T(8,128)(2,1)S(1)}, bf16[16,2048]{1,0:T(8,128)(2,1)S(1)}, u32[]{:S(2)}, u32[]{:S(2)}) %collective-permute-start.2) | collective-permute-done | bytes 65568 | tf_op jit(solution)/shard_map/ppermute | solution.py:339
  38.1 1.2 %shard_map.130 = (f32[8,6144]{1,0:T(8,128)S(1)}, bf16[128,2048]{1,0:T(8,128)(2,1)S(1)}) custom-call(bf16[16,8,768]{2,1,0:T(8,128)(2,1)S(1)} %all-to-all-done.1.second_ref, bf16[128,2048]{1,0:T(8,128)(2,1)} %collective-permute-done.low_hbm), custom_call_target="tpu_custom_call" | custom-call | flops 4000000000 | bytes 15625000 | tf_op jit(solution)/shard_map/pallas_call | solution.py:306
  39.4 0.3 copy-done.4
  39.7 0.7 %shard_map.132 = (bf16[64,512]{1,0:T(8,128)(2,1)S(1)}, f32[8,2048]{1,0:T(8,128)S(1)}) custom-call(f32[8,6144]{1,0:T(8,128)S(1)} %get-tuple-element.24.mod_ref, bf16[64,2048]{1,0:T(8,128)(2,1)S(1)} %shard_map.131.ctx_ref, f32[1,2048]{1,0:T(1,128)S(1)} %bitcast.10, bf16[2048,256]{1,0:T(8,128)(2,1)S(1)} %copy-done.3, bf16[2048,256]{1,0:T(8,128)(2,1)S(1)} %copy-done.4, ...), custom_call_target="tpu_custom_call" | custom-call | flops 4000000000 | bytes 15625000 | tf_op jit(solution)/shard_map/pallas_call | solution.py:306
  40.4 0.6 %collective-permute-start.7 = (bf16[64,512]{1,0:T(8,128)(2,1)S(1)}, bf16[64,512]{1,0:T(8,128)(2,1)S(1)}, u32[]{:S(2)}, u32[]{:S(2)}) collective-permute-start(bf16[64,512]{1,0:T(8,128)(2,1)S(1)} %get-tuple-element.32.x0_ref), channel_id=1, source_target_pairs={{0,6},{2,0},{4,2},{6,4},{1,7},{3,1},{5,3},{7,5},{8,14},{10,8},{12,... | collective-permute-start | bytes 196616 | tf_op jit(solution)/shard_map/ppermute | solution.py:339
  41.0 2.4 %collective-permute-start.6 = (bf16[64,512]{1,0:T(8,128)(2,1)S(1)}, bf16[64,512]{1,0:T(8,128)(2,1)S(1)}, u32[]{:S(2)}, u32[]{:S(2)}) collective-permute-start(bf16[64,512]{1,0:T(8,128)(2,1)S(1)} %get-tuple-element.32.x0_ref), channel_id=1, source_target_pairs={{0,4},{2,6},{4,0},{6,2},{1,5},{3,7},{5,1},{7,3},{8,12},{10,14},{12... | collective-permute-start | bytes 196616 | tf_op jit(solution)/shard_map/ppermute | solution.py:339
  43.4 1.8 %collective-permute-start.5 = (bf16[64,512]{1,0:T(8,128)(2,1)S(1)}, bf16[64,512]{1,0:T(8,128)(2,1)S(1)}, u32[]{:S(2)}, u32[]{:S(2)}) collective-permute-start(bf16[64,512]{1,0:T(8,128)(2,1)S(1)} %get-tuple-element.32.x0_ref), channel_id=1, source_target_pairs={{0,2},{2,4},{4,6},{6,0},{1,3},{3,5},{5,7},{7,1},{8,10},{10,12},{12... | collective-permute-start | bytes 196616 | tf_op jit(solution)/shard_map/ppermute | solution.py:339
  45.2 0.1 fusion.1
  45.5 0.2 fusion
  45.8 3.8 %shard_map.133 = (bf16[3,8,96,128]{3,2,1,0:T(8,128)(2,1)S(1)}, bf16[544,256]{1,0:T(8,128)(2,1)S(1)}, bf16[544,256]{1,0:T(8,128)(2,1)S(1)}) custom-call(bf16[128,2048]{1,0:T(8,128)(2,1)S(1)} %get-tuple-element.21.low_ref, bf16[288,2048]{1,0:T(8,128)(2,1)S(1)} %copy-done, bf16[128,2048]{1,0:T(8,128)(2,1)S(1)} %collective-permute-done.1.high_ref, ...), custom_call_target="tpu_custom_call" | custom-call | flops 6000000000 | bytes 23437500 | tf_op jit(solution)/shard_map/pallas_call | solution.py:306
  49.7 6.0 %shard_map.134 = bf16[288,2048]{1,0:T(8,128)(2,1)} custom-call(f32[1,8]{1,0:T(1,128)S(1)} %bitcast.14, bf16[3,8,96,128]{3,2,1,0:T(8,128)(2,1)S(1)} %get-tuple-element.29.q_ref, bf16[544,256]{1,0:T(8,128)(2,1)S(1)} %get-tuple-element.30.k_ref, bf16[544,256]{1,0:T(8,128)(2,1)S(1)} %get-tuple-element.31.v_ref, bf16[64,512]{1,0:T(8,128)(2,1)S(1)} %get-tuple-element.32.x0_ref, ...), custom_call_target="tpu_custom_call" | custom-call | flops 3000000000 | bytes 11718750 | tf_op jit(solution)/shard_map/pallas_call | solution.py:306
  (34 shorter events, 0.5 us)
Async XLA Ops:
  1.8 18.5 %all-to-all-start = ((bf16[16,8,768]{2,1,0:T(8,128)(2,1)}), bf16[16,8,768]{2,1,0:T(8,128)(2,1)S(1)}, u32[]{:S(2)}, u32[]{:S(2)}) async-start(bf16[16,8,768]{2,1,0:T(8,128)(2,1)} %shard_map.127), calls=%async_computation | async-start | bytes 393216 | tf_op jit(solution)/shard_map/all_to_all | solution.py:42
  12.6 25.5 %collective-permute-start = (bf16[128,2048]{1,0:T(8,128)(2,1)}, bf16[128,2048]{1,0:T(8,128)(2,1)}, u32[]{:S(2)}, u32[]{:S(2)}) collective-permute-start(bf16[128,2048]{1,0:T(8,128)(2,1)} %get-tuple-element.20), channel_id=1, source_target_pairs={{0,1},{1,2},{2,3},{3,4},{4,5},{5,6},{6,7},{7,8},{8,9},{9,10},{10,1... | collective-permute-start | bytes 1572872 | tf_op jit(solution)/shard_map/ppermute | solution.py:395
  14.9 30.9 %collective-permute-start.1 = (bf16[128,2048]{1,0:T(8,128)(2,1)}, bf16[128,2048]{1,0:T(8,128)(2,1)S(1)}, u32[]{:S(2)}, u32[]{:S(2)}) collective-permute-start(bf16[128,2048]{1,0:T(8,128)(2,1)} %get-tuple-element.22), channel_id=1, source_target_pairs={{1,0},{2,1},{3,2},{4,3},{5,4},{6,5},{7,6},{8,7},{9,8},{10,9},{11,1... | collective-permute-start | bytes 1572872 | tf_op jit(solution)/shard_map/ppermute | solution.py:396
  21.0 17.0 %all-to-all-start.1 = ((bf16[16,8,768]{2,1,0:T(8,128)(2,1)}), bf16[16,8,768]{2,1,0:T(8,128)(2,1)S(1)}, u32[]{:S(2)}, u32[]{:S(2)}) async-start(bf16[16,8,768]{2,1,0:T(8,128)(2,1)} %get-tuple-element.19), calls=%async_computation.1 | async-start | bytes 393216 | tf_op jit(solution)/shard_map/all_to_all | solution.py:42
  28.4 6.7 %collective-permute-start.4 = (bf16[16,2048]{1,0:T(8,128)(2,1)S(1)}, bf16[16,2048]{1,0:T(8,128)(2,1)S(1)}, u32[]{:S(2)}, u32[]{:S(2)}) collective-permute-start(bf16[16,2048]{1,0:T(8,128)(2,1)S(1)} %get-tuple-element.25.c0_ref), channel_id=1, source_target_pairs={{0,24},{8,0},{16,8},{24,16},{1,25},{9,1},{17,9},{25,17},{2,26},{10... | collective-permute-start | bytes 196616 | tf_op jit(solution)/shard_map/ppermute | solution.py:339
  31.2 6.1 %collective-permute-start.3 = (bf16[16,2048]{1,0:T(8,128)(2,1)S(1)}, bf16[16,2048]{1,0:T(8,128)(2,1)S(1)}, u32[]{:S(2)}, u32[]{:S(2)}) collective-permute-start(bf16[16,2048]{1,0:T(8,128)(2,1)S(1)} %get-tuple-element.25.c0_ref), channel_id=1, source_target_pairs={{0,16},{8,24},{16,0},{24,8},{1,17},{9,25},{17,1},{25,9},{2,18},{10... | collective-permute-start | bytes 196616 | tf_op jit(solution)/shard_map/ppermute | solution.py:339
  32.0 5.9 %collective-permute-start.2 = (bf16[16,2048]{1,0:T(8,128)(2,1)S(1)}, bf16[16,2048]{1,0:T(8,128)(2,1)S(1)}, u32[]{:S(2)}, u32[]{:S(2)}) collective-permute-start(bf16[16,2048]{1,0:T(8,128)(2,1)S(1)} %get-tuple-element.25.c0_ref), channel_id=1, source_target_pairs={{0,8},{8,16},{16,24},{24,0},{1,9},{9,17},{17,25},{25,1},{2,10},{10... | collective-permute-start | bytes 196616 | tf_op jit(solution)/shard_map/ppermute | solution.py:339
  38.0 1.4 %copy-start.3 = (bf16[2048,256]{1,0:T(8,128)(2,1)S(1)}, bf16[2048,256]{1,0:T(8,128)(2,1)}, u32[]{:S(2)}) copy-start(bf16[2048,256]{1,0:T(8,128)(2,1)} %wk_ref.3) | copy-start | bytes 3145732
  38.0 1.7 %copy-start.4 = (bf16[2048,256]{1,0:T(8,128)(2,1)S(1)}, bf16[2048,256]{1,0:T(8,128)(2,1)}, u32[]{:S(2)}) copy-start(bf16[2048,256]{1,0:T(8,128)(2,1)} %wv_ref.3) | copy-start | bytes 3145732
  38.0 1.7 %copy-start.5 = (f32[2048]{0:T(1024)S(1)}, f32[2048]{0:T(1024)}, u32[]{:S(2)}) copy-start(f32[2048]{0:T(1024)} %param.18) | copy-start | bytes 24580
  38.0 1.7 %copy-start.6 = (f32[128]{0:T(128)S(1)}, f32[128]{0:T(128)}, u32[]{:S(2)}) copy-start(f32[128]{0:T(128)} %param.24) | copy-start | bytes 1540
  39.7 6.1 %copy-start = (bf16[288,2048]{1,0:T(8,128)(2,1)S(1)}, bf16[288,2048]{1,0:T(8,128)(2,1)}, u32[]{:S(2)}) copy-start(bf16[288,2048]{1,0:T(8,128)(2,1)} %lat_ref.1) | copy-start | bytes 3538948
  39.7 6.1 %copy-start.1 = (bf16[2048,1024]{1,0:T(8,128)(2,1)S(1)}, bf16[2048,1024]{1,0:T(8,128)(2,1)}, u32[]{:S(2)}) copy-start(bf16[2048,1024]{1,0:T(8,128)(2,1)} %wq_ref.1) | copy-start | bytes 12582916
  39.7 6.1 %copy-start.7 = (f32[128]{0:T(128)S(1)}, f32[128]{0:T(128)}, u32[]{:S(2)}) copy-start(f32[128]{0:T(128)} %param.23) | copy-start | bytes 1540
  40.4 9.3 %collective-permute-start.7 = (bf16[64,512]{1,0:T(8,128)(2,1)S(1)}, bf16[64,512]{1,0:T(8,128)(2,1)S(1)}, u32[]{:S(2)}, u32[]{:S(2)}) collective-permute-start(bf16[64,512]{1,0:T(8,128)(2,1)S(1)} %get-tuple-element.32.x0_ref), channel_id=1, source_target_pairs={{0,6},{2,0},{4,2},{6,4},{1,7},{3,1},{5,3},{7,5},{8,14},{10,8},{12,... | collective-permute-start | bytes 196616 | tf_op jit(solution)/shard_map/ppermute | solution.py:339
  41.0 8.6 %collective-permute-start.6 = (bf16[64,512]{1,0:T(8,128)(2,1)S(1)}, bf16[64,512]{1,0:T(8,128)(2,1)S(1)}, u32[]{:S(2)}, u32[]{:S(2)}) collective-permute-start(bf16[64,512]{1,0:T(8,128)(2,1)S(1)} %get-tuple-element.32.x0_ref), channel_id=1, source_target_pairs={{0,4},{2,6},{4,0},{6,2},{1,5},{3,7},{5,1},{7,3},{8,12},{10,14},{12... | collective-permute-start | bytes 196616 | tf_op jit(solution)/shard_map/ppermute | solution.py:339
  43.4 6.3 %collective-permute-start.5 = (bf16[64,512]{1,0:T(8,128)(2,1)S(1)}, bf16[64,512]{1,0:T(8,128)(2,1)S(1)}, u32[]{:S(2)}, u32[]{:S(2)}) collective-permute-start(bf16[64,512]{1,0:T(8,128)(2,1)S(1)} %get-tuple-element.32.x0_ref), channel_id=1, source_target_pairs={{0,2},{2,4},{4,6},{6,0},{1,3},{3,5},{5,7},{7,1},{8,10},{10,12},{12... | collective-permute-start | bytes 196616 | tf_op jit(solution)/shard_map/ppermute | solution.py:339
  45.8 3.9 %copy-start.2 = (bf16[1024,2048]{1,0:T(8,128)(2,1)S(1)}, bf16[1024,2048]{1,0:T(8,128)(2,1)}, u32[]{:S(2)}) copy-start(bf16[1024,2048]{1,0:T(8,128)(2,1)} %wo_ref.1) | copy-start | bytes 12582916
  45.8 3.9 %copy-start.8 = (f32[8]{0:T(128)S(1)}, f32[8]{0:T(128)}, u32[]{:S(2)}) copy-start(f32[8]{0:T(128)} %param.25) | copy-start | bytes 100
